TPU v7x, 32 devices: a whole 2x2x4 slice. The times are simulated.
32 devices in a mesh: sp: 8 (over z, core), tp: 4 (over y, x).
Axes of the slice: x: 2, y: 2, z: 4, core: 2. Of those that a mesh axis runs over, the one named last changes fastest.
Arguments:
- cotangent: bfloat16 [1024, 2048], P('sp'), may hold values from -6 to 6
- normed: bfloat16 [1024, 2048], P('sp'), may hold values from -6 to 6
- inverse_root_mean_square: float32 [1024], P('sp'), may hold values from 0.5 to 2
- expert_norm_scale: float32 [2048], replicated, may hold values from 0.1 to 1.9
- routes: int32 [1024, 2], P('sp'), may hold values from 0 to 7, all different within a row; in each aligned block of 128 rows (0 to 127, 128 to 255, ...) at most 64 rows name the same one
- route_probability_weight: float32 [1024, 2], P('sp'), may hold values from 0.2 to 1
- gate_weight: bfloat16 [8, 2048, 2048], P('sp', None, 'tp'), may hold values from -0.125 to 0.125
- up_weight: bfloat16 [8, 2048, 2048], P('sp', None, 'tp'), may hold values from -0.125 to 0.125
- down_weight: bfloat16 [8, 2048, 2048], P('sp', 'tp'), may hold values from -0.125 to 0.125
- recurrence_input: bfloat16 [1024, 1024], P('sp', 'tp'), may hold values from -6 to 6
- recurrence_gate_logits: bfloat16 [1024, 1024], P('sp', 'tp'), may hold values from -6 to 6
- input_gate_logits: bfloat16 [1024, 1024], P('sp', 'tp'), may hold values from -6 to 6
- channel_decay_weight: float32 [1024], P('tp'), may hold values from 3 to 20
- extra_log_decay: float32 [1024, 1024], P('sp', 'tp'), may hold values from -1 to 0
- output_matrix: bfloat16 [2048, 1024], P(None, 'tp'), may hold values from -0.1875 to 0.1875
Outputs:
- grad_gate: bfloat16 [8, 2048, 2048], P('sp', None, 'tp')
- grad_up: bfloat16 [8, 2048, 2048], P('sp', None, 'tp')
- grad_down: bfloat16 [8, 2048, 2048], P('sp', 'tp')
- grad_out_weight: float32 [2048, 1024], P('sp', 'tp')
- grad_rec_input: float32 [1024, 1024], P('sp', 'tp')
- grad_decay_gate: float32 [1024, 1024], P('sp', 'tp')
- grad_input_gate: float32 [1024, 1024], P('sp', 'tp')
Inputs may be any that keep to these rules, and one draw needn't show every extreme that they name: `routes`: each row names 2 different experts; among the rows of one device no expert is named more than 64 times.
All inputs are finite; a program needn't handle non-finite values.
Results may differ from a plain program's by a relative error of at most 0.025.
Values may be sent and summed in bfloat16 or wider, within the bound.
No kernel may reach another device: no remote copies, remote signals or barrier semaphores. Data moves between devices by JAX's collectives and lax.ppermute only.
A program may use at most 64 MiB of HBM per device.

v0:
```python
import functools

import jax
import jax.numpy as jnp
from jax import lax
from jax.experimental import pallas as pl
from jax.experimental.pallas import tpu as pltpu
from jax.sharding import PartitionSpec as P


F32, BF16 = jnp.float32, jnp.bfloat16
ROWS = (((0,), (0,)), ((), ()))
COLS = (((1,), (1,)), ((), ()))
PLAIN = (((1,), (0,)), ((), ()))


def dot(a, b, dims=PLAIN):
    return lax.dot_general(a, b, dims, preferred_element_type=F32)


def call(body, outs, *args, scalars=None, mib=24):
    vm = pl.BlockSpec(memory_space=pltpu.VMEM)
    sm = pl.BlockSpec(memory_space=pltpu.SMEM)
    ins = ([sm] if scalars is not None else []) + [vm] * len(args)
    if scalars is not None:
        args = (scalars,) + tuple(args)
    return pl.pallas_call(
        body,
        out_shape=outs,
        in_specs=ins,
        out_specs=jax.tree.map(lambda _: vm, outs),
        compiler_params=pltpu.CompilerParams(vmem_limit_bytes=mib << 20),
    )(*args)


def hbm(x):
    return pltpu.with_memory_space_constraint(x, pltpu.HBM)


def swap(x, axis, m):
    n = lax.axis_size(axis)
    return lax.ppermute(x, axis, [(i, i ^ m) for i in range(n)])


def wide(t, width):
    return pl.ds(pl.multiple_of(t * width, width), width)


def landing(groups, cap, s, routes_ref):
    tok = routes_ref.shape[1]
    e0, e1 = routes_ref[0:1, :], routes_ref[1:2, :]
    ids = lax.broadcasted_iota(jnp.int32, (groups, tok), 0)
    hit0, hit1 = ids == e0, ids == e1
    member = jnp.where(hit0 | hit1, 1.0, 0.0).astype(BF16)
    upper = (
        lax.broadcasted_iota(jnp.int32, (tok, tok), 0)
        < lax.broadcasted_iota(jnp.int32, (tok, tok), 1)
    )
    rank = dot(member, jnp.where(upper, 1.0, 0.0).astype(BF16))
    r0 = jnp.sum(jnp.where(hit0, rank, 0.0), axis=0, keepdims=True).astype(jnp.int32)
    r1 = jnp.sum(jnp.where(hit1, rank, 0.0), axis=0, keepdims=True).astype(jnp.int32)
    return (e0 ^ s) * cap + r0, (e1 ^ s) * cap + r1


def picked(groups, cap, place_ref, routes_ref):
    land0, land1 = landing(groups, cap, place_ref[0], routes_ref)
    slots = lax.broadcasted_iota(jnp.int32, (groups * cap, routes_ref.shape[1]), 0)
    in0, in1 = slots == land0, slots == land1
    return in0, in1, jnp.where(in0 | in1, 1.0, 0.0).astype(BF16)


def scales(in0, in1, weight_ref):
    weight = jnp.where(in0, weight_ref[0:1, :], 0.0) + jnp.where(in1, weight_ref[1:2, :], 0.0)
    return jnp.sum(weight, axis=1, keepdims=True)


def far_body(groups, near, tps, cap, place_ref, routes_ref, weight_ref, normed_ref, cot_ref, *outs):
    count = groups - near
    xs, ys, whole = outs[:count], outs[count : 2 * count], outs[2 * count :]
    quarter = wide(place_ref[1], normed_ref.shape[1] // tps)
    in0, in1, pick = picked(groups, cap, place_ref, routes_ref)
    cut = near * cap
    x = dot(pick[cut:, :], normed_ref[:, quarter]).astype(BF16)
    y = dot(pick[cut:, :], cot_ref[:, quarter]) * scales(in0[cut:, :], in1[cut:, :], weight_ref)
    y = y.astype(BF16)
    for m in range(count):
        xs[m][...] = x[m * cap : (m + 1) * cap, :]
        ys[m][...] = y[m * cap : (m + 1) * cap, :]
    x = dot(pick[2 * cap : cut, :], normed_ref[...]).astype(BF16)
    for m, out in enumerate(whole):
        out[...] = x[m * cap : (m + 1) * cap, :]


def near_body(groups, near, cap, place_ref, routes_ref, weight_ref, normed_ref, cot_ref, edge_ref, *outs):
    in0, in1, pick = picked(groups, cap, place_ref, routes_ref)
    cut = near * cap
    edge = edge_ref[...]
    x = dot(pick[: 2 * cap, :], normed_ref[...]).astype(BF16)
    y = dot(pick[:cut, :], cot_ref[...]) * scales(in0[:cut, :], in1[:cut, :], weight_ref)
    y = y.astype(BF16)
    for m, out in enumerate(outs):
        out[:cap, :] = y[m * cap : (m + 1) * cap, :]
        out[cap : cap + 8, :] = jnp.zeros((8, out.shape[1]), BF16)
        out[cap : cap + 8, : edge.shape[1]] = edge
        if m < 2:
            out[cap + 8 :, :] = x[m * cap : (m + 1) * cap, :]


def edges_body(cap, *refs):
    out_ref = refs[-1]
    for m, r in enumerate(refs[:-1]):
        out_ref[8 * m : 8 * m + 8, :] = r[cap : cap + 8, : out_ref.shape[1]]


def join_body(cap, *refs):
    for m, r in enumerate(refs[:-1]):
        refs[-1][m * cap : (m + 1) * cap, :] = r[:cap, :]


def column(row):
    n = row.shape[1]
    eye = (
        lax.broadcasted_iota(jnp.int32, (n, n), 0)
        == lax.broadcasted_iota(jnp.int32, (n, n), 1)
    )
    return jnp.sum(jnp.where(eye, row, 0.0), axis=1, keepdims=True)


def slots_body(groups, cap, place_ref, routes_ref, out_ref):
    land0, land1 = landing(groups, cap, place_ref[0], routes_ref)
    land0 = column(land0.astype(F32)).astype(jnp.int32)
    land1 = column(land1.astype(F32)).astype(jnp.int32)
    slots = lax.broadcasted_iota(jnp.int32, out_ref.shape, 1)
    out_ref[...] = jnp.where((slots == land0) | (slots == land1), 1.0, 0.0).astype(BF16)


def shifted(x, by, fill, down):
    pad = jnp.full((by, x.shape[1]), fill, x.dtype)
    return (
        jnp.concatenate([pad, x[:-by, :]], axis=0)
        if down
        else jnp.concatenate([x[by:, :], pad], axis=0)
    )


def scan(keep, value, forward):
    by = 1
    while by < keep.shape[0]:
        value = keep * shifted(value, by, 0.0, forward) + value
        keep = keep * shifted(keep, by, 1.0, forward)
        by *= 2
    return keep, value


def forward_body(keep_ref, driven_ref, cum_ref, state_ref, tail_ref, edge_ref):
    keep = keep_ref[...]
    cum, state = scan(keep, driven_ref[...], True)
    tail = shifted(keep, 1, 1.0, False)
    by = 1
    while by < keep.shape[0]:
        tail = tail * shifted(tail, by, 1.0, False)
        by *= 2
    cum_ref[...] = cum
    state_ref[...] = state
    tail_ref[...] = tail
    edge = [cum[-1:, :], state[-1:, :], keep[:1, :] * tail[:1, :]]
    edge_ref[...] = jnp.concatenate(pair_of(edge), axis=0).astype(BF16)


def pair_of(rows):
    high = [r.astype(BF16).astype(F32) for r in rows]
    both = high + [r - h for r, h in zip(rows, high)]
    return both + [jnp.zeros_like(rows[0])] * (8 - len(both))


def enter_body(groups, place_ref, cum_ref, state_ref, k1_ref, k2_ref, edges_ref, hidden_ref, kk_ref, coef_ref):
    s = place_ref[0]
    chan = cum_ref.shape[1]
    edges = []
    for m in range(groups):
        e = edges_ref[8 * m : 8 * m + 8, :].astype(F32)
        edges.append(e[:3, :] + e[3:6, :])

    def edge(i, row):
        out = edges[0][row : row + 1, :]
        for m in range(1, groups):
            out = jnp.where((s ^ m) == i, edges[m][row : row + 1, :], out)
        return out

    state_in = jnp.zeros((1, chan), F32)
    product = jnp.ones((1, chan), F32)
    coefs = []
    for i in range(groups):
        state_in = jnp.where(i < s, state_in * edge(i, 0) + edge(i, 1), state_in)
        coefs.append(jnp.where(i > s, product, 0.0))
        product = jnp.where(i > s, product * edge(i, 2), product)
    state = state_ref[...] + cum_ref[...] * state_in
    hidden_ref[...] = state.astype(BF16)
    before = jnp.concatenate([state_in, state[:-1, :]], axis=0)
    kk_ref[...] = before * k1_ref[...] + k2_ref[...]
    for m in range(groups):
        out = jnp.zeros((1, chan), F32)
        for i in range(groups):
            out = jnp.where((s ^ m) == i, coefs[i], out)
        coef_ref[m : m + 1, :] = out


def put(out_ref, first, t, tps, pieces):
    for i, piece in enumerate(pieces):
        rows, width = piece.shape
        out_ref[first : first + rows, wide(t ^ (i % tps), width)] = piece[...]
        if i % tps == tps - 1:
            first += rows


def hidden_body(near, tps, cap, place_ref, gate_ref, up_ref, *rest):
    refs, (act_ref, swish_ref, slope_ref, x_ref) = rest[:-4], rest[-4:]
    for m in range(near):
        first = cap + 8 if m < 2 else 0
        x_ref[m * cap : (m + 1) * cap, :] = refs[m][first : first + cap, :]
    put(x_ref, near * cap, place_ref[1], tps, refs[near:])
    x = x_ref[...]
    gate = dot(x, gate_ref[...])
    up = dot(x, up_ref[...])
    sigma = jax.nn.sigmoid(gate)
    swish = gate * sigma
    act_ref[...] = (swish * up).astype(BF16)
    swish_ref[...] = swish
    slope_ref[...] = up * sigma * (1.0 + gate * (1.0 - sigma))


def back_body(first, near, tps, cap, place_ref, gate_ref, up_ref, down_ref, swish_ref, slope_ref, *rest):
    count = len(rest) - 3 - tps
    refs, (y_ref, dg_ref, du_ref, *outs) = rest[:count], rest[count:]
    t = place_ref[1]
    if near:
        for m in range(near):
            y_ref[m * cap : (m + 1) * cap, :] = refs[m][:cap, :]
    else:
        put(y_ref, 0, t, tps, refs)
    rows = y_ref.shape[0]
    at = slice(first, first + rows)
    d_act = dot(y_ref[...], down_ref[...], COLS)
    dg = (d_act * slope_ref[at, :]).astype(BF16)
    du = (d_act * swish_ref[at, :]).astype(BF16)
    dg_ref[...] = dg
    du_ref[...] = du
    width = gate_ref.shape[0] // tps

    def part(j):
        cols = wide(t ^ j, width)
        return dot(dg, gate_ref[cols, :], COLS) + dot(du, up_ref[cols, :], COLS)

    if tps != 4:
        for j in range(tps):
            outs[j][...] = part(j).astype(BF16)
        return
    half = rows // 2
    send_a, send_b, keep_a, keep_b = outs
    last = part(3).astype(BF16)
    send_a[half:, :] = last[:half, :]
    send_b[half:, :] = last[half:, :]
    one = part(1)
    send_a[:half, :] = one[:half, :].astype(BF16)
    keep_b[half:, :] = one[half:, :]
    two = part(2)
    send_b[:half, :] = two[half:, :].astype(BF16)
    keep_a[half:, :] = two[:half, :]
    mine = part(0)
    keep_a[:half, :] = mine[:half, :]
    keep_b[:half, :] = mine[half:, :]


def middle_body(keep_a, keep_b, got_a, got_b, stay_a, stay_b, go_a, go_b):
    half = stay_a.shape[0]
    for keep, got, stay, go in ((keep_a, got_a, stay_a, go_a), (keep_b, got_b, stay_b, go_b)):
        stay[...] = keep[:half, :] + got[:half, :].astype(F32)
        go[...] = (keep[half:, :] + got[half:, :].astype(F32)).astype(BF16)


def last_body(cap, stay_a, stay_b, got_a, got_b, *outs):
    half = len(outs) // 2
    a = (stay_a[...] + got_a[...].astype(F32)).astype(BF16)
    b = (stay_b[...] + got_b[...].astype(F32)).astype(BF16)
    for m, o in enumerate(outs):
        i = m % half
        o[...] = (a if m < half else b)[i * cap : (i + 1) * cap, :]


def grads_body(split, act_ref, x_ref, dg0_ref, du0_ref, y0_ref, dg1_ref, du1_ref, y1_ref, gg_ref, gu_ref, gd_ref):
    x0, x1 = x_ref[:split, :], x_ref[split:, :]
    gg_ref[...] = (dot(x0, dg0_ref[...], ROWS) + dot(x1, dg1_ref[...], ROWS)).astype(BF16)
    gu_ref[...] = (dot(x0, du0_ref[...], ROWS) + dot(x1, du1_ref[...], ROWS)).astype(BF16)
    a0, a1 = act_ref[:split, :], act_ref[split:, :]
    gd_ref[...] = (dot(a0, y0_ref[...], ROWS) + dot(a1, y1_ref[...], ROWS)).astype(BF16)


def sums_body(cap, *refs):
    count = refs[0].shape[0] // cap
    pieces, outs = refs[:-count], refs[-count:]
    total = pieces[0][...].astype(F32)
    for p in pieces[1:]:
        total = total + p[...].astype(F32)
    for m, o in enumerate(outs):
        o[...] = total[m * cap : (m + 1) * cap, :].astype(BF16)


def combine_body(slots_ref, *rest):
    blocks, out_ref = rest[:-1], rest[-1]
    rows = jnp.concatenate([b[...] for b in blocks], axis=0)
    out_ref[...] = dot(slots_ref[...], rows).astype(BF16)


def mix_body(tps, place_ref, inv_ref, gain_ref, normed_ref, cot_ref, mat_ref, keep_ref, *rest):
    pieces, (grad_ref, *strips, dn_ref, mix_ref) = rest[:tps], rest[tps:]
    s, t = place_ref[0], place_ref[1]
    for j in range(tps):
        dn_ref[:, wide(t ^ j, pieces[j].shape[1])] = pieces[j][...]
    dn = dn_ref[...].astype(F32)
    normed = normed_ref[...].astype(F32)
    gain = gain_ref[...]
    stat = jnp.sum(dn * normed, axis=1, keepdims=True) * (1.0 / dn.shape[1])
    mix = cot_ref[...].astype(F32) + column(inv_ref[...]) * (gain * dn - (normed / gain) * stat)
    mix = mix.astype(BF16)
    mix_ref[...] = mix
    keep = keep_ref[...]
    d_state = dot(mix, mat_ref[...])
    _, grad = scan(shifted(keep, 1, 1.0, False), d_state, False)
    grad_ref[...] = grad
    late = jnp.concatenate(pair_of([keep[:1, :] * grad[:1, :]]), axis=0).astype(BF16)
    tok, chan = keep.shape
    width = strips[0].shape[1]
    for m, out in enumerate(strips):
        if width % 128:
            both = mix_ref[:, wide((s ^ m) // 2, 2 * width)].astype(F32)
            odd = ((s ^ m) & 1) == 1
            out[:tok, :] = jnp.where(odd, both[:, width:], both[:, :width]).astype(BF16)
        else:
            out[:tok, :] = mix_ref[:, wide(s ^ m, width)]
        out[tok:, :] = jnp.zeros((8, width), BF16)
        out[tok:, :chan] = late


def final_body(groups, tok, coef_ref, grad_ref, tail_ref, opened_ref, kk_ref, slope_ref, hid_even_ref, hid_odd_ref, *rest):
    strips, (out_ref, rec_ref, decay_ref, gate_ref) = rest[:groups], rest[groups:]
    chan = grad_ref.shape[1]
    enter = jnp.zeros((1, chan), F32)
    weight = jnp.zeros(out_ref.shape, F32)
    for m in range(groups):
        hidden = (hid_odd_ref if m % 2 else hid_even_ref)[m // 2 * tok : (m // 2 + 1) * tok, :]
        late = strips[m][tok : tok + 8, :chan].astype(F32)
        enter = enter + coef_ref[m : m + 1, :] * (late[0:1, :] + late[1:2, :])
        weight = weight + dot(strips[m][:tok, :], hidden, ROWS)
    out_ref[...] = weight
    total = grad_ref[...] + tail_ref[...] * enter
    rec_ref[...] = total * opened_ref[...]
    decay_ref[...] = total * kk_ref[...]
    gate_ref[...] = total * slope_ref[...]


def sds(shape, dtype):
    return jax.ShapeDtypeStruct(shape, dtype)


def shards(
    cotangent,
    normed,
    inverse_root_mean_square,
    expert_norm_scale,
    routes,
    route_probability_weight,
    gate_weight,
    up_weight,
    down_weight,
    recurrence_input,
    recurrence_gate_logits,
    input_gate_logits,
    channel_decay_weight,
    extra_log_decay,
    output_matrix,
):
    tok, features = normed.shape
    groups, tps = lax.axis_size("sp"), lax.axis_size("tp")
    cap = 2 * routes.shape[1] * tok // groups
    rows = groups * cap
    width = features // tps
    s, t = lax.axis_index("sp"), lax.axis_index("tp")
    place = jnp.stack([s, t]).astype(jnp.int32)
    gate_w, up_w, down_w = gate_weight[0], up_weight[0], down_weight[0]
    hid = gate_w.shape[1]
    chan = output_matrix.shape[1]

    near = min(4, groups)
    routes_t, weights_t = routes.T, route_probability_weight.T
    plane = sds((tok, chan), F32)
    thin = sds((tok, chan), BF16)

    far = groups - near
    block = sds((cap, width), BF16)
    packed = call(
        functools.partial(far_body, groups, near, tps, cap),
        [block] * (2 * far) + [sds((cap, features), BF16)] * (near - 2),
        hbm(routes_t),
        hbm(weights_t),
        hbm(normed),
        hbm(cotangent),
        scalars=place,
    )
    packed, recurrence_input, recurrence_gate_logits, input_gate_logits, extra_log_decay, channel_decay_weight = (
        lax.optimization_barrier(
            (packed, recurrence_input, recurrence_gate_logits, input_gate_logits, extra_log_decay, channel_decay_weight)
        )
    )
    xs = [swap(x, "sp", near + m) for m, x in enumerate(packed[:far])]
    ys = [swap(y, "sp", near + m) for m, y in enumerate(packed[far : 2 * far])]
    close_x = [swap(x, "sp", 2 + m) for m, x in enumerate(packed[2 * far :])]

    retain = jax.nn.sigmoid(recurrence_gate_logits.astype(F32))
    admit = jax.nn.sigmoid(input_gate_logits.astype(F32))
    signal = recurrence_input.astype(F32)
    speed = -8.0 * jax.nn.softplus(-channel_decay_weight)[None, :]
    log_keep = retain * speed + extra_log_decay
    keep = jnp.exp(log_keep)
    scale_in = jnp.sqrt(-jnp.expm1(2.0 * log_keep))
    opened = scale_in * admit
    driven = opened * signal
    slope = driven * (1.0 - admit)
    decay = speed * retain * (1.0 - retain)
    k1 = keep * decay
    k2 = -admit * signal * keep * keep / scale_in * decay
    cum, state_loc, tail, edge = call(
        forward_body, [plane, plane, plane, sds((8, chan), BF16)], keep, driven
    )

    close_y = call(
        functools.partial(near_body, groups, near, cap),
        [sds(((cap if m > 1 else 2 * cap) + 8, features), BF16) for m in range(near)],
        hbm(routes_t),
        hbm(weights_t),
        hbm(normed),
        hbm(cotangent),
        edge,
        scalars=place,
    )
    close_y = [close_y[0]] + [swap(c, "sp", m) for m, c in enumerate(close_y) if m]
    edges = call(functools.partial(edges_body, cap), sds((8 * near, chan), BF16), *close_y)
    step = near
    while step < groups:
        edges = jnp.concatenate([edges, swap(edges, "sp", step)], axis=0)
        step *= 2

    def spread(blocks):
        mine = call(
            functools.partial(join_body, cap), sds((len(blocks) * cap, width), BF16), *blocks
        )
        return [mine] + [swap(mine, "tp", j) for j in range(1, tps)]

    xp = spread(xs)
    half = far // 2
    yp = spread(ys[:half]) + spread(ys[half:])

    hidden, kk, coef = call(
        functools.partial(enter_body, groups),
        [thin, plane, sds((groups, chan), F32)],
        cum,
        state_loc,
        k1,
        k2,
        edges,
        scalars=place,
    )
    slots = call(
        functools.partial(slots_body, groups, cap), sds((tok, rows), BF16), routes_t, scalars=place
    )

    wide_rows = sds((rows, hid), F32)
    thin_rows = sds((rows, hid), BF16)
    full_rows = sds((rows, features), BF16)
    act, swish, bend, x_all = call(
        functools.partial(hidden_body, near, tps, cap),
        [thin_rows, wide_rows, wide_rows, full_rows],
        gate_w,
        up_w,
        *close_y[:2],
        *close_x,
        *xp,
        scalars=place,
    )

    def back(first, count, refs):
        n = count * cap
        piece = sds((n, width), BF16)
        keep_rows = sds((n, width), F32)
        return call(
            functools.partial(back_body, first, 0 if first else near, tps, cap),
            [sds((n, features), BF16), sds((n, hid), BF16), sds((n, hid), BF16)]
            + ([piece, piece, keep_rows, keep_rows] if tps == 4 else [piece] * tps),
            gate_w,
            up_w,
            down_w,
            swish,
            bend,
            *refs,
            scalars=place,
        )

    y1, dg1, du1, *parts1 = back(near * cap, far, yp)
    y0, dg0, du0, *parts0 = back(0, near, close_y)
    grads = call(
        functools.partial(grads_body, near * cap),
        [sds((features, hid), BF16), sds((features, hid), BF16), sds((hid, features), BF16)],
        act,
        x_all,
        dg0,
        du0,
        y0,
        dg1,
        du1,
        y1,
    )

    def reduced(parts, count):
        outs = [block] * count
        if tps != 4:
            got = [parts[0]] + [swap(parts[j], "tp", j) for j in range(1, tps)]
            return call(functools.partial(sums_body, cap), outs, *got)
        send_a, send_b, keep_a, keep_b = parts
        got_a, got_b = swap(send_a, "tp", 1), swap(send_b, "tp", 2)
        n = count * cap // 2
        stay_a, stay_b, go_a, go_b = call(
            middle_body,
            [sds((n, width), F32)] * 2 + [sds((n, width), BF16)] * 2,
            keep_a,
            keep_b,
            got_a,
            got_b,
        )
        got_a, got_b = swap(go_a, "tp", 2), swap(go_b, "tp", 1)
        return call(functools.partial(last_body, cap), outs, stay_a, stay_b, got_a, got_b)

    summed = reduced(parts1, far)
    summed = list(reduced(parts0, near)) + list(summed)
    blocks = [summed[0]] + [swap(b, "sp", m) for m, b in enumerate(summed) if m]
    grad_gate, grad_up, grad_down = grads
    hid_even = jnp.concatenate(
        [hidden] + [swap(hidden, "sp", m) for m in range(2, groups, 2)], axis=0
    )
    hid_odd = swap(hid_even, "sp", 1)

    d_norm = call(combine_body, sds((tok, width), BF16), slots, *blocks)
    norms = [d_norm] + [swap(d_norm, "tp", j) for j in range(1, tps)]
    strip = features // groups
    grad_loc, *strips = call(
        functools.partial(mix_body, tps),
        [plane] + [sds((tok + 8, strip), BF16)] * groups + [sds((tok, features), BF16)] * 2,
        inverse_root_mean_square[None, :],
        expert_norm_scale[None, :],
        normed,
        cotangent,
        output_matrix,
        keep,
        *norms,
        scalars=place,
    )[:-2]
    strips = [strips[0]] + [swap(c, "sp", m) for m, c in enumerate(strips) if m]
    grad_out_weight, grad_rec, grad_decay, grad_input = call(
        functools.partial(final_body, groups, tok),
        [sds((strip, chan), F32), plane, plane, plane],
        coef,
        grad_loc,
        tail,
        opened,
        kk,
        slope,
        hid_even,
        hid_odd,
        *strips,
    )
    return (
        grad_gate[None],
        grad_up[None],
        grad_down[None],
        grad_out_weight,
        grad_rec,
        grad_decay,
        grad_input,
    )


def solution(mesh):
    return jax.shard_map(
        shards,
        mesh=mesh,
        in_specs=(
            P("sp", None),
            P("sp", None),
            P("sp"),
            P(),
            P("sp", None),
            P("sp", None),
            P("sp", None, "tp"),
            P("sp", None, "tp"),
            P("sp", "tp", None),
            P("sp", "tp"),
            P("sp", "tp"),
            P("sp", "tp"),
            P("tp"),
            P("sp", "tp"),
            P(None, "tp"),
        ),
        out_specs=(
            P("sp", None, "tp"),
            P("sp", None, "tp"),
            P("sp", "tp", None),
            P("sp", "tp"),
            P("sp", "tp"),
            P("sp", "tp"),
            P("sp", "tp"),
        ),
        check_vma=False,
    )
```

profile of v0, /device:TPU:0, one launch (start us, length us, event | category | flops | bytes accessed | tf_op | source)
XLA Modules:
  0.0 125.5 jit_solution(8200350785427868604)
XLA Ops:
  0.7 2.0 %shard_map.198 = (bf16[64,512]{1,0:T(8,128)(2,1)S(1)}, bf16[64,512]{1,0:T(8,128)(2,1)S(1)}, bf16[64,512]{1,0:T(8,128)(2,1)S(1)}, bf16[64,512]{1,0:T(8,128)(2,1)S...) custom-call(s32[2]{0:T(128)S(1)} %pad_add_fusion.place_ref, ...), custom_call_target="tpu_custom_call" | custom-call | tf_op jit(solution)/shard_map/pallas_call | solution.py:27
  2.7 4.1 %collective-permute-start.3 = (bf16[64,512]{1,0:T(8,128)(2,1)S(1)}, bf16[64,512]{1,0:T(8,128)(2,1)S(1)}, u32[]{:S(2)}, u32[]{:S(2)}) collective-permute-start(bf16[64,512]{1,0:T(8,128)(2,1)S(1)} %get-tuple-element.113), channel_id=1, source_target_pairs={{0,16},{4,20},{8,24},{12,28},{16,0},{20,4},{24,8},{28,12},{1,17},{... | collective-permute-start | bytes 196616 | tf_op jit(solution)/shard_map/ppermute | solution.py:42
  6.8 3.1 %collective-permute-start.5 = (bf16[64,512]{1,0:T(8,128)(2,1)S(1)}, bf16[64,512]{1,0:T(8,128)(2,1)S(1)}, u32[]{:S(2)}, u32[]{:S(2)}) collective-permute-start(bf16[64,512]{1,0:T(8,128)(2,1)S(1)} %get-tuple-element.115), channel_id=1, source_target_pairs={{0,24},{4,28},{8,16},{12,20},{16,8},{20,12},{24,0},{28,4},{1,25},{... | collective-permute-start | bytes 196616 | tf_op jit(solution)/shard_map/ppermute | solution.py:42
  12.0 2.0 %shard_map.200 = (bf16[136,2048]{1,0:T(8,128)(2,1)S(1)}, bf16[136,2048]{1,0:T(8,128)(2,1)S(1)}, bf16[72,2048]{1,0:T(8,128)(2,1)S(1)}, bf16[72,2048]{1,0:T(8,128)(2,1)S(1)}) custom-call(s32[2]{0:T(128)S(1)} %pad_add_fusion.place_ref, s32[2,128]{1,0:T(2,128)} %bitcast.21, f32[2,128]{1,0:T(2,128)} %bitcast.26, bf16[128,2048]{1,0:T(8,128)(2,1)} %normed_ref.5, ...), custom_call_target="tpu_custom_call" | custom-call | tf_op jit(solution)/shard_map/pallas_call | solution.py:27
  14.7 2.4 %collective-permute-start.13 = (bf16[64,512]{1,0:T(8,128)(2,1)S(1)}, bf16[64,512]{1,0:T(8,128)(2,1)S(1)}, u32[]{:S(2)}, u32[]{:S(2)}) collective-permute-start(bf16[64,512]{1,0:T(8,128)(2,1)S(1)} %get-tuple-element.127), channel_id=1, source_target_pairs={{0,20},{4,16},{8,28},{12,24},{16,4},{20,0},{24,12},{28,8},{1,21},{... | collective-permute-start | bytes 196616 | tf_op jit(solution)/shard_map/ppermute | solution.py:42
  17.1 2.0 %collective-permute-start.6 = (bf16[64,512]{1,0:T(8,128)(2,1)S(1)}, bf16[64,512]{1,0:T(8,128)(2,1)S(1)}, u32[]{:S(2)}, u32[]{:S(2)}) collective-permute-start(bf16[64,512]{1,0:T(8,128)(2,1)S(1)} %get-tuple-element.116), channel_id=1, source_target_pairs={{0,28},{4,24},{8,20},{12,16},{16,12},{20,8},{24,4},{28,0},{1,29},{... | collective-permute-start | bytes 196616 | tf_op jit(solution)/shard_map/ppermute | solution.py:42
  19.1 4.5 %collective-permute-start.17 = (bf16[64,512]{1,0:T(8,128)(2,1)S(1)}, bf16[64,512]{1,0:T(8,128)(2,1)S(1)}, u32[]{:S(2)}, u32[]{:S(2)}) collective-permute-start(bf16[64,512]{1,0:T(8,128)(2,1)S(1)} %get-tuple-element.128), channel_id=1, source_target_pairs={{0,24},{4,28},{8,16},{12,20},{16,8},{20,12},{24,0},{28,4},{1,25},{... | collective-permute-start | bytes 196616 | tf_op jit(solution)/shard_map/ppermute | solution.py:42
  24.8 2.1 %collective-permute-done.6.refs_3_ = bf16[64,512]{1,0:T(8,128)(2,1)S(1)} collective-permute-done((bf16[64,512]{1,0:T(8,128)(2,1)S(1)}, bf16[64,512]{1,0:T(8,128)(2,1)S(1)}, u32[]{:S(2)}, u32[]{:S(2)}) %collective-permute-start.6) | collective-permute-done | bytes 65568 | tf_op jit(solution)/shard_map/ppermute | solution.py:42
  26.9 1.9 %collective-permute-start.14 = (bf16[128,512]{1,0:T(8,128)(2,1)S(1)}, bf16[128,512]{1,0:T(8,128)(2,1)S(1)}, u32[]{:S(2)}, u32[]{:S(2)}) collective-permute-start(bf16[128,512]{1,0:T(8,128)(2,1)S(1)} %shard_map.204.rest_0_), channel_id=1, source_target_pairs={{0,1},{1,0},{2,3},{3,2},{4,5},{5,4},{6,7},{7,6},{8,9},{9,8},{10,11... | collective-permute-start | bytes 393224 | tf_op jit(solution)/shard_map/ppermute | solution.py:42
  29.3 1.6 %collective-permute-start.15 = (bf16[128,512]{1,0:T(8,128)(2,1)S(1)}, bf16[128,512]{1,0:T(8,128)(2,1)S(1)}, u32[]{:S(2)}, u32[]{:S(2)}) collective-permute-start(bf16[128,512]{1,0:T(8,128)(2,1)S(1)} %shard_map.204.rest_0_), channel_id=1, source_target_pairs={{0,2},{1,3},{2,0},{3,1},{4,6},{5,7},{6,4},{7,5},{8,10},{9,11},{10,... | collective-permute-start | bytes 393224 | tf_op jit(solution)/shard_map/ppermute | solution.py:42
  30.9 1.8 %collective-permute-start.16 = (bf16[128,512]{1,0:T(8,128)(2,1)S(1)}, bf16[128,512]{1,0:T(8,128)(2,1)S(1)}, u32[]{:S(2)}, u32[]{:S(2)}) collective-permute-start(bf16[128,512]{1,0:T(8,128)(2,1)S(1)} %shard_map.204.rest_0_), channel_id=1, source_target_pairs={{0,3},{1,2},{2,1},{3,0},{4,7},{5,6},{6,5},{7,4},{8,11},{9,10},{10,... | collective-permute-start | bytes 393224 | tf_op jit(solution)/shard_map/ppermute | solution.py:42
  33.3 3.8 %collective-permute-done.15.rest_2_ = bf16[128,512]{1,0:T(8,128)(2,1)S(1)} collective-permute-done((bf16[128,512]{1,0:T(8,128)(2,1)S(1)}, bf16[128,512]{1,0:T(8,128)(2,1)S(1)}, u32[]{:S(2)}, u32[]{:S(2)}) %collective-permute-start.15) | collective-permute-done | bytes 131104 | tf_op jit(solution)/shard_map/ppermute | solution.py:42
  41.6 3.7 %collective-permute-done.7.rest_5_ = bf16[256,512]{1,0:T(8,128)(2,1)S(1)} collective-permute-done((bf16[256,512]{1,0:T(8,128)(2,1)S(1)}, bf16[256,512]{1,0:T(8,128)(2,1)S(1)}, u32[]{:S(2)}, u32[]{:S(2)}) %collective-permute-start.7) | collective-permute-done | bytes 262176 | tf_op jit(solution)/shard_map/ppermute | solution.py:42
  45.3 4.4 %collective-permute-done.8.rest_6_ = bf16[256,512]{1,0:T(8,128)(2,1)S(1)} collective-permute-done((bf16[256,512]{1,0:T(8,128)(2,1)S(1)}, bf16[256,512]{1,0:T(8,128)(2,1)S(1)}, u32[]{:S(2)}, u32[]{:S(2)}) %collective-permute-start.8) | collective-permute-done | bytes 262176 | tf_op jit(solution)/shard_map/ppermute | solution.py:42
  53.2 3.2 %shard_map.202 = (bf16[512,512]{1,0:T(8,128)(2,1)S(1)}, f32[512,512]{1,0:T(8,128)S(1)}, f32[512,512]{1,0:T(8,128)S(1)}, bf16[512,2048]{1,0:T(8,128)(2,1)S(1)}) custom-call(s32[2]{0:T(128)S(1)} %pad_add_fusion.place_ref, bf16[2048,512]{1,0:T(8,128)(2,1)S(1)} %bitcast.12, bf16[2048,512]{1,0:T(8,128)(2,1)S(1)} %bitcast.15, ...), custom_call_target="tpu_custom_call" | custom-call | tf_op jit(solution)/shard_map/pallas_call | solution.py:27
  56.5 2.1 %collective-permute-done.21.rest_7_ = bf16[128,512]{1,0:T(8,128)(2,1)S(1)} collective-permute-done((bf16[128,512]{1,0:T(8,128)(2,1)S(1)}, bf16[128,512]{1,0:T(8,128)(2,1)S(1)}, u32[]{:S(2)}, u32[]{:S(2)}) %collective-permute-start.21) | collective-permute-done | bytes 131104 | tf_op jit(solution)/shard_map/ppermute | solution.py:42
  58.6 2.5 %shard_map.206 = (bf16[256,2048]{1,0:T(8,128)(2,1)S(1)}, bf16[256,512]{1,0:T(8,128)(2,1)S(1)}, bf16[256,512]{1,0:T(8,128)(2,1)S(1)}, bf16[256,512]{1,0:T(8,128)(...) custom-call(s32[2]{0:T(128)S(1)} %pad_add_fusion.place_ref, ...), custom_call_target="tpu_custom_call" | custom-call | tf_op jit(solution)/shard_map/pallas_call | solution.py:27
  62.2 2.5 %shard_map.203 = (bf16[256,2048]{1,0:T(8,128)(2,1)S(1)}, bf16[256,512]{1,0:T(8,128)(2,1)S(1)}, bf16[256,512]{1,0:T(8,128)(2,1)S(1)}, bf16[256,512]{1,0:T(8,128)(...) custom-call(s32[2]{0:T(128)S(1)} %pad_add_fusion.place_ref, ...), custom_call_target="tpu_custom_call" | custom-call | tf_op jit(solution)/shard_map/pallas_call | solution.py:27
  67.8 3.0 %collective-permute-start.22 = (bf16[32,256]{1,0:T(8,128)(2,1)S(1)}, bf16[32,256]{1,0:T(8,128)(2,1)S(1)}, u32[]{:S(2)}, u32[]{:S(2)}) collective-permute-start(bf16[32,256]{1,0:T(8,128)(2,1)S(1)} %shard_map.208), channel_id=1, source_target_pairs={{0,16},{4,20},{8,24},{12,28},{16,0},{20,4},{24,8},{28,12},{1,17},{... | collective-permute-start | bytes 49160 | tf_op jit(solution)/shard_map/ppermute | solution.py:42
  70.7 1.7 %collective-permute-done.22 = bf16[32,256]{1,0:T(8,128)(2,1)S(1)} collective-permute-done((bf16[32,256]{1,0:T(8,128)(2,1)S(1)}, bf16[32,256]{1,0:T(8,128)(2,1)S(1)}, u32[]{:S(2)}, u32[]{:S(2)}) %collective-permute-start.22) | collective-permute-done | bytes 16416 | tf_op jit(solution)/shard_map/ppermute | solution.py:42
  76.1 2.6 %collective-permute-start.42 = (bf16[128,256]{1,0:T(8,128)(2,1)S(1)}, bf16[128,256]{1,0:T(8,128)(2,1)S(1)}, u32[]{:S(2)}, u32[]{:S(2)}) collective-permute-start(bf16[128,256]{1,0:T(8,128)(2,1)S(1)} %get-tuple-element.166), channel_id=1, source_target_pairs={{0,16},{4,20},{8,24},{12,28},{16,0},{20,4},{24,8},{28,12},{1,17},{... | collective-permute-start | bytes 196616 | tf_op jit(solution)/shard_map/ppermute | solution.py:42
  84.4 2.4 %collective-permute-start.36 = (bf16[64,512]{1,0:T(8,128)(2,1)S(1)}, bf16[64,512]{1,0:T(8,128)(2,1)S(1)}, u32[]{:S(2)}, u32[]{:S(2)}) collective-permute-start(bf16[64,512]{1,0:T(8,128)(2,1)S(1)} %get-tuple-element.161), channel_id=1, source_target_pairs={{0,24},{4,28},{8,16},{12,20},{16,8},{20,12},{24,0},{28,4},{1,25},{... | collective-permute-start | bytes 196616 | tf_op jit(solution)/shard_map/ppermute | solution.py:42
  86.8 2.4 %collective-permute-start.37 = (bf16[64,512]{1,0:T(8,128)(2,1)S(1)}, bf16[64,512]{1,0:T(8,128)(2,1)S(1)}, u32[]{:S(2)}, u32[]{:S(2)}) collective-permute-start(bf16[64,512]{1,0:T(8,128)(2,1)S(1)} %get-tuple-element.162), channel_id=1, source_target_pairs={{0,28},{4,24},{8,20},{12,16},{16,12},{20,8},{24,4},{28,0},{1,29},{... | collective-permute-start | bytes 196616 | tf_op jit(solution)/shard_map/ppermute | solution.py:42
  89.3 3.8 %collective-permute-done.34.rest_4_ = bf16[64,512]{1,0:T(8,128)(2,1)S(1)} collective-permute-done((bf16[64,512]{1,0:T(8,128)(2,1)S(1)}, bf16[64,512]{1,0:T(8,128)(2,1)S(1)}, u32[]{:S(2)}, u32[]{:S(2)}) %collective-permute-start.34) | collective-permute-done | bytes 65568 | tf_op jit(solution)/shard_map/ppermute | solution.py:42
  93.3 2.0 %collective-permute-start.44 = (bf16[512,256]{1,0:T(8,128)(2,1)S(1)}, bf16[512,256]{1,0:T(8,128)(2,1)S(1)}, u32[]{:S(2)}, u32[]{:S(2)}) collective-permute-start(bf16[512,256]{1,0:T(8,128)(2,1)S(1)} %constant_dynamic-update-slice_fusion.hid_even_ref), channel_id=1, source_target_pairs={{0,4},{4,0},{8,12},{12,8},{16,20},{20,16},{24,28},{28,24},{1,5},{5... | collective-permute-start | bytes 786440 | tf_op jit(solution)/shard_map/ppermute | solution.py:42
  101.5 2.9 %collective-permute-done.38.rest_1_ = bf16[128,512]{1,0:T(8,128)(2,1)S(1)} collective-permute-done((bf16[128,512]{1,0:T(8,128)(2,1)S(1)}, bf16[128,512]{1,0:T(8,128)(2,1)S(1)}, u32[]{:S(2)}, u32[]{:S(2)}) %collective-permute-start.38) | collective-permute-done | bytes 131104 | tf_op jit(solution)/shard_map/ppermute | solution.py:42
  104.3 3.0 %collective-permute-done.39.rest_2_ = bf16[128,512]{1,0:T(8,128)(2,1)S(1)} collective-permute-done((bf16[128,512]{1,0:T(8,128)(2,1)S(1)}, bf16[128,512]{1,0:T(8,128)(2,1)S(1)}, u32[]{:S(2)}, u32[]{:S(2)}) %collective-permute-start.39) | collective-permute-done | bytes 131104 | tf_op jit(solution)/shard_map/ppermute | solution.py:42
  107.4 2.3 %shard_map.216 = (f32[128,256]{1,0:T(8,128)S(1)}, bf16[136,256]{1,0:T(8,128)(2,1)S(1)}, bf16[136,256]{1,0:T(8,128)(2,1)S(1)}, bf16[136,256]{1,0:T(8,128)(2,1)S(1...) custom-call(s32[2]{0:T(128)S(1)} %pad_add_fusion.place_ref, ...), custom_call_target="tpu_custom_call" | custom-call | tf_op jit(solution)/shard_map/pallas_call | solution.py:27
  109.9 1.7 %collective-permute-start.47 = (bf16[136,256]{1,0:T(8,128)(2,1)S(1)}, bf16[136,256]{1,0:T(8,128)(2,1)S(1)}, u32[]{:S(2)}, u32[]{:S(2)}) collective-permute-start(bf16[136,256]{1,0:T(8,128)(2,1)S(1)} %get-tuple-element.170), channel_id=1, source_target_pairs={{0,12},{4,8},{8,4},{12,0},{16,28},{20,24},{24,20},{28,16},{1,13},{... | collective-permute-start | bytes 208904 | tf_op jit(solution)/shard_map/ppermute | solution.py:42
  111.5 1.7 %collective-permute-start.48 = (bf16[136,256]{1,0:T(8,128)(2,1)S(1)}, bf16[136,256]{1,0:T(8,128)(2,1)S(1)}, u32[]{:S(2)}, u32[]{:S(2)}) collective-permute-start(bf16[136,256]{1,0:T(8,128)(2,1)S(1)} %get-tuple-element.171), channel_id=1, source_target_pairs={{0,16},{4,20},{8,24},{12,28},{16,0},{20,4},{24,8},{28,12},{1,17},{... | collective-permute-start | bytes 208904 | tf_op jit(solution)/shard_map/ppermute | solution.py:42
  114.0 2.7 %collective-permute-start.50 = (bf16[136,256]{1,0:T(8,128)(2,1)S(1)}, bf16[136,256]{1,0:T(8,128)(2,1)S(1)}, u32[]{:S(2)}, u32[]{:S(2)}) collective-permute-start(bf16[136,256]{1,0:T(8,128)(2,1)S(1)} %get-tuple-element.173), channel_id=1, source_target_pairs={{0,24},{4,28},{8,16},{12,20},{16,8},{20,12},{24,0},{28,4},{1,25},{... | collective-permute-start | bytes 208904 | tf_op jit(solution)/shard_map/ppermute | solution.py:42
  117.7 5.5 %shard_map.207 = (bf16[2048,512]{1,0:T(8,128)(2,1)}, bf16[2048,512]{1,0:T(8,128)(2,1)}, bf16[512,2048]{1,0:T(8,128)(2,1)}) custom-call(bf16[512,512]{1,0:T(8,128)(2,1)S(1)} %get-tuple-element.117.act_ref, bf16[512,2048]{1,0:T(8,128)(2,1)S(1)} %get-tuple-element.118.x_ref, bf16[256,512]{1,0:T(8,128)(2,1)S(1)} %get-tuple-element.123.dg0_ref, ...), custom_call_target="tpu_custom_call" | custom-call | tf_op jit(solution)/shard_map/pallas_call | solution.py:27
  (118 shorter events, 37.4 us)
Async XLA Ops:
  2.7 12.1 %collective-permute-start.3 = (bf16[64,512]{1,0:T(8,128)(2,1)S(1)}, bf16[64,512]{1,0:T(8,128)(2,1)S(1)}, u32[]{:S(2)}, u32[]{:S(2)}) collective-permute-start(bf16[64,512]{1,0:T(8,128)(2,1)S(1)} %get-tuple-element.113), channel_id=1, source_target_pairs={{0,16},{4,20},{8,24},{12,28},{16,0},{20,4},{24,8},{28,12},{1,17},{... | collective-permute-start | bytes 196616 | tf_op jit(solution)/shard_map/ppermute | solution.py:42
  6.8 10.3 %collective-permute-start.4 = (bf16[64,512]{1,0:T(8,128)(2,1)S(1)}, bf16[64,512]{1,0:T(8,128)(2,1)S(1)}, u32[]{:S(2)}, u32[]{:S(2)}) collective-permute-start(bf16[64,512]{1,0:T(8,128)(2,1)S(1)} %get-tuple-element.114), channel_id=1, source_target_pairs={{0,20},{4,16},{8,28},{12,24},{16,4},{20,0},{24,12},{28,8},{1,21},{... | collective-permute-start | bytes 196616 | tf_op jit(solution)/shard_map/ppermute | solution.py:42
  6.8 10.3 %collective-permute-start.5 = (bf16[64,512]{1,0:T(8,128)(2,1)S(1)}, bf16[64,512]{1,0:T(8,128)(2,1)S(1)}, u32[]{:S(2)}, u32[]{:S(2)}) collective-permute-start(bf16[64,512]{1,0:T(8,128)(2,1)S(1)} %get-tuple-element.115), channel_id=1, source_target_pairs={{0,24},{4,28},{8,16},{12,20},{16,8},{20,12},{24,0},{28,4},{1,25},{... | collective-permute-start | bytes 196616 | tf_op jit(solution)/shard_map/ppermute | solution.py:42
  9.9 9.2 %collective-permute-start.12 = (bf16[64,512]{1,0:T(8,128)(2,1)S(1)}, bf16[64,512]{1,0:T(8,128)(2,1)S(1)}, u32[]{:S(2)}, u32[]{:S(2)}) collective-permute-start(bf16[64,512]{1,0:T(8,128)(2,1)S(1)} %get-tuple-element.126), channel_id=1, source_target_pairs={{0,16},{4,20},{8,24},{12,28},{16,0},{20,4},{24,8},{28,12},{1,17},{... | collective-permute-start | bytes 196616 | tf_op jit(solution)/shard_map/ppermute | solution.py:42
  14.0 38.7 %collective-permute-start = (bf16[136,2048]{1,0:T(8,128)(2,1)S(1)}, bf16[136,2048]{1,0:T(8,128)(2,1)S(1)}, u32[]{:S(2)}, u32[]{:S(2)}) collective-permute-start(bf16[136,2048]{1,0:T(8,128)(2,1)S(1)} %get-tuple-element.110), channel_id=1, source_target_pairs={{0,4},{4,0},{8,12},{12,8},{16,20},{20,16},{24,28},{28,24},{1,5},{5... | collective-permute-start | bytes 1671176 | tf_op jit(solution)/shard_map/ppermute | solution.py:42
  14.7 8.9 %collective-permute-start.13 = (bf16[64,512]{1,0:T(8,128)(2,1)S(1)}, bf16[64,512]{1,0:T(8,128)(2,1)S(1)}, u32[]{:S(2)}, u32[]{:S(2)}) collective-permute-start(bf16[64,512]{1,0:T(8,128)(2,1)S(1)} %get-tuple-element.127), channel_id=1, source_target_pairs={{0,20},{4,16},{8,28},{12,24},{16,4},{20,0},{24,12},{28,8},{1,21},{... | collective-permute-start | bytes 196616 | tf_op jit(solution)/shard_map/ppermute | solution.py:42
  17.1 22.5 %collective-permute-start.1 = (bf16[64,2048]{1,0:T(8,128)(2,1)S(1)}, bf16[64,2048]{1,0:T(8,128)(2,1)S(1)}, u32[]{:S(2)}, u32[]{:S(2)}) collective-permute-start(bf16[64,2048]{1,0:T(8,128)(2,1)S(1)} %get-tuple-element.111), channel_id=1, source_target_pairs={{0,8},{4,12},{8,0},{12,4},{16,24},{20,28},{24,16},{28,20},{1,9},{5... | collective-permute-start | bytes 786440 | tf_op jit(solution)/shard_map/ppermute | solution.py:42
  17.1 9.8 %collective-permute-start.6 = (bf16[64,512]{1,0:T(8,128)(2,1)S(1)}, bf16[64,512]{1,0:T(8,128)(2,1)S(1)}, u32[]{:S(2)}, u32[]{:S(2)}) collective-permute-start(bf16[64,512]{1,0:T(8,128)(2,1)S(1)} %get-tuple-element.116), channel_id=1, source_target_pairs={{0,28},{4,24},{8,20},{12,16},{16,12},{20,8},{24,4},{28,0},{1,29},{... | collective-permute-start | bytes 196616 | tf_op jit(solution)/shard_map/ppermute | solution.py:42
  19.1 10.2 %collective-permute-start.17 = (bf16[64,512]{1,0:T(8,128)(2,1)S(1)}, bf16[64,512]{1,0:T(8,128)(2,1)S(1)}, u32[]{:S(2)}, u32[]{:S(2)}) collective-permute-start(bf16[64,512]{1,0:T(8,128)(2,1)S(1)} %get-tuple-element.128), channel_id=1, source_target_pairs={{0,24},{4,28},{8,16},{12,20},{16,8},{20,12},{24,0},{28,4},{1,25},{... | collective-permute-start | bytes 196616 | tf_op jit(solution)/shard_map/ppermute | solution.py:42
  29.3 7.8 %collective-permute-start.15 = (bf16[128,512]{1,0:T(8,128)(2,1)S(1)}, bf16[128,512]{1,0:T(8,128)(2,1)S(1)}, u32[]{:S(2)}, u32[]{:S(2)}) collective-permute-start(bf16[128,512]{1,0:T(8,128)(2,1)S(1)} %shard_map.204.rest_0_), channel_id=1, source_target_pairs={{0,2},{1,3},{2,0},{3,1},{4,6},{5,7},{6,4},{7,5},{8,10},{9,11},{10,... | collective-permute-start | bytes 393224 | tf_op jit(solution)/shard_map/ppermute | solution.py:42
  33.3 8.3 %collective-permute-start.2 = (bf16[64,2048]{1,0:T(8,128)(2,1)S(1)}, bf16[64,2048]{1,0:T(8,128)(2,1)S(1)}, u32[]{:S(2)}, u32[]{:S(2)}) collective-permute-start(bf16[64,2048]{1,0:T(8,128)(2,1)S(1)} %get-tuple-element.112), channel_id=1, source_target_pairs={{0,12},{4,8},{8,4},{12,0},{16,28},{20,24},{24,20},{28,16},{1,13},{... | collective-permute-start | bytes 786440 | tf_op jit(solution)/shard_map/ppermute | solution.py:42
  37.1 8.3 %collective-permute-start.7 = (bf16[256,512]{1,0:T(8,128)(2,1)S(1)}, bf16[256,512]{1,0:T(8,128)(2,1)S(1)}, u32[]{:S(2)}, u32[]{:S(2)}) collective-permute-start(bf16[256,512]{1,0:T(8,128)(2,1)S(1)} %shard_map.201.rest_4_), channel_id=1, source_target_pairs={{0,1},{1,0},{2,3},{3,2},{4,5},{5,4},{6,7},{7,6},{8,9},{9,8},{10,11... | collective-permute-start | bytes 786440 | tf_op jit(solution)/shard_map/ppermute | solution.py:42
  38.4 11.3 %collective-permute-start.8 = (bf16[256,512]{1,0:T(8,128)(2,1)S(1)}, bf16[256,512]{1,0:T(8,128)(2,1)S(1)}, u32[]{:S(2)}, u32[]{:S(2)}) collective-permute-start(bf16[256,512]{1,0:T(8,128)(2,1)S(1)} %shard_map.201.rest_4_), channel_id=1, source_target_pairs={{0,2},{1,3},{2,0},{3,1},{4,6},{5,7},{6,4},{7,5},{8,10},{9,11},{10,... | collective-permute-start | bytes 786440 | tf_op jit(solution)/shard_map/ppermute | solution.py:42
  39.6 11.5 %collective-permute-start.9 = (bf16[256,512]{1,0:T(8,128)(2,1)S(1)}, bf16[256,512]{1,0:T(8,128)(2,1)S(1)}, u32[]{:S(2)}, u32[]{:S(2)}) collective-permute-start(bf16[256,512]{1,0:T(8,128)(2,1)S(1)} %shard_map.201.rest_4_), channel_id=1, source_target_pairs={{0,3},{1,2},{2,1},{3,0},{4,7},{5,6},{6,5},{7,4},{8,11},{9,10},{10,... | collective-permute-start | bytes 786440 | tf_op jit(solution)/shard_map/ppermute | solution.py:42
  41.6 20.6 %collective-permute-start.10 = (bf16[72,2048]{1,0:T(8,128)(2,1)S(1)}, bf16[72,2048]{1,0:T(8,128)(2,1)S(1)}, u32[]{:S(2)}, u32[]{:S(2)}) collective-permute-start(bf16[72,2048]{1,0:T(8,128)(2,1)S(1)} %get-tuple-element.121), channel_id=1, source_target_pairs={{0,8},{4,12},{8,0},{12,4},{16,24},{20,28},{24,16},{28,20},{1,9},{5... | collective-permute-start | bytes 884744 | tf_op jit(solution)/shard_map/ppermute | solution.py:42
  45.3 16.9 %collective-permute-start.11 = (bf16[72,2048]{1,0:T(8,128)(2,1)S(1)}, bf16[72,2048]{1,0:T(8,128)(2,1)S(1)}, u32[]{:S(2)}, u32[]{:S(2)}) collective-permute-start(bf16[72,2048]{1,0:T(8,128)(2,1)S(1)} %get-tuple-element.122), channel_id=1, source_target_pairs={{0,12},{4,8},{8,4},{12,0},{16,28},{20,24},{24,20},{28,16},{1,13},{... | collective-permute-start | bytes 884744 | tf_op jit(solution)/shard_map/ppermute | solution.py:42
  61.1 12.9 %collective-permute-start.30 = (bf16[256,512]{1,0:T(8,128)(2,1)S(1)}, bf16[256,512]{1,0:T(8,128)(2,1)S(1)}, u32[]{:S(2)}, u32[]{:S(2)}) collective-permute-start(bf16[256,512]{1,0:T(8,128)(2,1)S(1)} %get-tuple-element.153), channel_id=1, source_target_pairs={{0,1},{1,0},{2,3},{3,2},{4,5},{5,4},{6,7},{7,6},{8,9},{9,8},{10,11... | collective-permute-start | bytes 786440 | tf_op jit(solution)/shard_map/ppermute | solution.py:42
  61.7 12.2 %collective-permute-start.31 = (bf16[256,512]{1,0:T(8,128)(2,1)S(1)}, bf16[256,512]{1,0:T(8,128)(2,1)S(1)}, u32[]{:S(2)}, u32[]{:S(2)}) collective-permute-start(bf16[256,512]{1,0:T(8,128)(2,1)S(1)} %get-tuple-element.154), channel_id=1, source_target_pairs={{0,2},{1,3},{2,0},{3,1},{4,6},{5,7},{6,4},{7,5},{8,10},{9,11},{10,... | collective-permute-start | bytes 786440 | tf_op jit(solution)/shard_map/ppermute | solution.py:42
  64.7 11.4 %collective-permute-start.23 = (bf16[256,512]{1,0:T(8,128)(2,1)S(1)}, bf16[256,512]{1,0:T(8,128)(2,1)S(1)}, u32[]{:S(2)}, u32[]{:S(2)}) collective-permute-start(bf16[256,512]{1,0:T(8,128)(2,1)S(1)} %get-tuple-element.141), channel_id=1, source_target_pairs={{0,1},{1,0},{2,3},{3,2},{4,5},{5,4},{6,7},{7,6},{8,9},{9,8},{10,11... | collective-permute-start | bytes 786440 | tf_op jit(solution)/shard_map/ppermute | solution.py:42
  66.2 12.5 %collective-permute-start.24 = (bf16[256,512]{1,0:T(8,128)(2,1)S(1)}, bf16[256,512]{1,0:T(8,128)(2,1)S(1)}, u32[]{:S(2)}, u32[]{:S(2)}) collective-permute-start(bf16[256,512]{1,0:T(8,128)(2,1)S(1)} %get-tuple-element.142), channel_id=1, source_target_pairs={{0,2},{1,3},{2,0},{3,1},{4,6},{5,7},{6,4},{7,5},{8,10},{9,11},{10,... | collective-permute-start | bytes 786440 | tf_op jit(solution)/shard_map/ppermute | solution.py:42
  76.1 8.2 %collective-permute-start.42 = (bf16[128,256]{1,0:T(8,128)(2,1)S(1)}, bf16[128,256]{1,0:T(8,128)(2,1)S(1)}, u32[]{:S(2)}, u32[]{:S(2)}) collective-permute-start(bf16[128,256]{1,0:T(8,128)(2,1)S(1)} %get-tuple-element.166), channel_id=1, source_target_pairs={{0,16},{4,20},{8,24},{12,28},{16,0},{20,4},{24,8},{28,12},{1,17},{... | collective-permute-start | bytes 196616 | tf_op jit(solution)/shard_map/ppermute | solution.py:42
  81.4 7.8 %collective-permute-start.43 = (bf16[128,256]{1,0:T(8,128)(2,1)S(1)}, bf16[128,256]{1,0:T(8,128)(2,1)S(1)}, u32[]{:S(2)}, u32[]{:S(2)}) collective-permute-start(bf16[128,256]{1,0:T(8,128)(2,1)S(1)} %get-tuple-element.166), channel_id=1, source_target_pairs={{0,24},{4,28},{8,16},{12,20},{16,8},{20,12},{24,0},{28,4},{1,25},{... | collective-permute-start | bytes 196616 | tf_op jit(solution)/shard_map/ppermute | solution.py:42
  82.8 10.3 %collective-permute-start.34 = (bf16[64,512]{1,0:T(8,128)(2,1)S(1)}, bf16[64,512]{1,0:T(8,128)(2,1)S(1)}, u32[]{:S(2)}, u32[]{:S(2)}) collective-permute-start(bf16[64,512]{1,0:T(8,128)(2,1)S(1)} %get-tuple-element.159), channel_id=1, source_target_pairs={{0,16},{4,20},{8,24},{12,28},{16,0},{20,4},{24,8},{28,12},{1,17},{... | collective-permute-start | bytes 196616 | tf_op jit(solution)/shard_map/ppermute | solution.py:42
  84.3 8.9 %collective-permute-start.35 = (bf16[64,512]{1,0:T(8,128)(2,1)S(1)}, bf16[64,512]{1,0:T(8,128)(2,1)S(1)}, u32[]{:S(2)}, u32[]{:S(2)}) collective-permute-start(bf16[64,512]{1,0:T(8,128)(2,1)S(1)} %get-tuple-element.160), channel_id=1, source_target_pairs={{0,20},{4,16},{8,28},{12,24},{16,4},{20,0},{24,12},{28,8},{1,21},{... | collective-permute-start | bytes 196616 | tf_op jit(solution)/shard_map/ppermute | solution.py:42
  84.4 8.9 %collective-permute-start.36 = (bf16[64,512]{1,0:T(8,128)(2,1)S(1)}, bf16[64,512]{1,0:T(8,128)(2,1)S(1)}, u32[]{:S(2)}, u32[]{:S(2)}) collective-permute-start(bf16[64,512]{1,0:T(8,128)(2,1)S(1)} %get-tuple-element.161), channel_id=1, source_target_pairs={{0,24},{4,28},{8,16},{12,20},{16,8},{20,12},{24,0},{28,4},{1,25},{... | collective-permute-start | bytes 196616 | tf_op jit(solution)/shard_map/ppermute | solution.py:42
  86.8 9.4 %collective-permute-start.37 = (bf16[64,512]{1,0:T(8,128)(2,1)S(1)}, bf16[64,512]{1,0:T(8,128)(2,1)S(1)}, u32[]{:S(2)}, u32[]{:S(2)}) collective-permute-start(bf16[64,512]{1,0:T(8,128)(2,1)S(1)} %get-tuple-element.162), channel_id=1, source_target_pairs={{0,28},{4,24},{8,20},{12,16},{16,12},{20,8},{24,4},{28,0},{1,29},{... | collective-permute-start | bytes 196616 | tf_op jit(solution)/shard_map/ppermute | solution.py:42
  93.3 19.9 %collective-permute-start.44 = (bf16[512,256]{1,0:T(8,128)(2,1)S(1)}, bf16[512,256]{1,0:T(8,128)(2,1)S(1)}, u32[]{:S(2)}, u32[]{:S(2)}) collective-permute-start(bf16[512,256]{1,0:T(8,128)(2,1)S(1)} %constant_dynamic-update-slice_fusion.hid_even_ref), channel_id=1, source_target_pairs={{0,4},{4,0},{8,12},{12,8},{16,20},{20,16},{24,28},{28,24},{1,5},{5... | collective-permute-start | bytes 786440 | tf_op jit(solution)/shard_map/ppermute | solution.py:42
  98.7 8.6 %collective-permute-start.39 = (bf16[128,512]{1,0:T(8,128)(2,1)S(1)}, bf16[128,512]{1,0:T(8,128)(2,1)S(1)}, u32[]{:S(2)}, u32[]{:S(2)}) collective-permute-start(bf16[128,512]{1,0:T(8,128)(2,1)S(1)} %shard_map.215.rest_0_), channel_id=1, source_target_pairs={{0,2},{1,3},{2,0},{3,1},{4,6},{5,7},{6,4},{7,5},{8,10},{9,11},{10,... | collective-permute-start | bytes 393224 | tf_op jit(solution)/shard_map/ppermute | solution.py:42
  109.9 13.4 %collective-permute-start.47 = (bf16[136,256]{1,0:T(8,128)(2,1)S(1)}, bf16[136,256]{1,0:T(8,128)(2,1)S(1)}, u32[]{:S(2)}, u32[]{:S(2)}) collective-permute-start(bf16[136,256]{1,0:T(8,128)(2,1)S(1)} %get-tuple-element.170), channel_id=1, source_target_pairs={{0,12},{4,8},{8,4},{12,0},{16,28},{20,24},{24,20},{28,16},{1,13},{... | collective-permute-start | bytes 208904 | tf_op jit(solution)/shard_map/ppermute | solution.py:42
  111.5 11.7 %collective-permute-start.48 = (bf16[136,256]{1,0:T(8,128)(2,1)S(1)}, bf16[136,256]{1,0:T(8,128)(2,1)S(1)}, u32[]{:S(2)}, u32[]{:S(2)}) collective-permute-start(bf16[136,256]{1,0:T(8,128)(2,1)S(1)} %get-tuple-element.171), channel_id=1, source_target_pairs={{0,16},{4,20},{8,24},{12,28},{16,0},{20,4},{24,8},{28,12},{1,17},{... | collective-permute-start | bytes 208904 | tf_op jit(solution)/shard_map/ppermute | solution.py:42
  113.2 11.0 %collective-permute-start.49 = (bf16[136,256]{1,0:T(8,128)(2,1)S(1)}, bf16[136,256]{1,0:T(8,128)(2,1)S(1)}, u32[]{:S(2)}, u32[]{:S(2)}) collective-permute-start(bf16[136,256]{1,0:T(8,128)(2,1)S(1)} %get-tuple-element.172), channel_id=1, source_target_pairs={{0,20},{4,16},{8,28},{12,24},{16,4},{20,0},{24,12},{28,8},{1,21},{... | collective-permute-start | bytes 208904 | tf_op jit(solution)/shard_map/ppermute | solution.py:42
  114.0 10.2 %collective-permute-start.50 = (bf16[136,256]{1,0:T(8,128)(2,1)S(1)}, bf16[136,256]{1,0:T(8,128)(2,1)S(1)}, u32[]{:S(2)}, u32[]{:S(2)}) collective-permute-start(bf16[136,256]{1,0:T(8,128)(2,1)S(1)} %get-tuple-element.173), channel_id=1, source_target_pairs={{0,24},{4,28},{8,16},{12,20},{16,8},{20,12},{24,0},{28,4},{1,25},{... | collective-permute-start | bytes 208904 | tf_op jit(solution)/shard_map/ppermute | solution.py:42
  (29 other events, 401.0 us)
where the time goes:
time: 126 us; the launch traced here: 125 us
  starting transfers between devices  66.7 us (53%)
  waiting for transfers between devices  32.4 us (26%)
  Pallas kernels  23.5 us (19%)
  other arithmetic  1.98 us (2%)
    ppermute x52, starting transfers between devices, swap(): return lax.ppermute(x, axis, [(i, i ^ m) for i in range(n)])  66.7 us
    ppermute x52, waiting for transfers between devices, swap(): return lax.ppermute(x, axis, [(i, i ^ m) for i in range(n)])  32.4 us
    pallas_call x20, Pallas kernels, call(): pl.pallas_call(body, out_shape=outs, in_specs=ins, out_specs=jax.tree.map...  23.5 us
  transfers between devices with their start and end apart: 52, of which 15 were waited for; matrix products, arithmetic and copies ran while one was open for 2% of the time, Pallas kernels for 16%

commit v1 on v0

--- a/solution.py
+++ b/solution.py
@@ -18,7 +18,7 @@
     return lax.dot_general(a, b, dims, preferred_element_type=F32)
 
 
-def call(body, outs, *args, scalars=None, mib=24):
+def call(body, outs, *args, scalars=None, mib=24, scratch=()):
     vm = pl.BlockSpec(memory_space=pltpu.VMEM)
     sm = pl.BlockSpec(memory_space=pltpu.SMEM)
     ins = ([sm] if scalars is not None else []) + [vm] * len(args)
@@ -29,6 +29,7 @@
         out_shape=outs,
         in_specs=ins,
         out_specs=jax.tree.map(lambda _: vm, outs),
+        scratch_shapes=[pltpu.VMEM(x.shape, x.dtype) for x in scratch],
         compiler_params=pltpu.CompilerParams(vmem_limit_bytes=mib << 20),
     )(*args)
 
@@ -205,20 +206,18 @@
         coef_ref[m : m + 1, :] = out
 
 
-def put(out_ref, first, t, tps, pieces):
-    for i, piece in enumerate(pieces):
+def put(out_ref, t, at, pieces):
+    for (first, j), piece in zip(at, pieces):
         rows, width = piece.shape
-        out_ref[first : first + rows, wide(t ^ (i % tps), width)] = piece[...]
-        if i % tps == tps - 1:
-            first += rows
-
-
-def hidden_body(near, tps, cap, place_ref, gate_ref, up_ref, *rest):
+        out_ref[first : first + rows, wide(t ^ j, width)] = piece[...]
+
+
+def hidden_body(near, cap, at, place_ref, gate_ref, up_ref, *rest):
     refs, (act_ref, swish_ref, slope_ref, x_ref) = rest[:-4], rest[-4:]
     for m in range(near):
         first = cap + 8 if m < 2 else 0
         x_ref[m * cap : (m + 1) * cap, :] = refs[m][first : first + cap, :]
-    put(x_ref, near * cap, place_ref[1], tps, refs[near:])
+    put(x_ref, place_ref[1], at, refs[near:])
     x = x_ref[...]
     gate = dot(x, gate_ref[...])
     up = dot(x, up_ref[...])
@@ -229,7 +228,7 @@
     slope_ref[...] = up * sigma * (1.0 + gate * (1.0 - sigma))
 
 
-def back_body(first, near, tps, cap, place_ref, gate_ref, up_ref, down_ref, swish_ref, slope_ref, *rest):
+def back_body(first, near, tps, cap, at, place_ref, gate_ref, up_ref, down_ref, swish_ref, slope_ref, *rest):
     count = len(rest) - 3 - tps
     refs, (y_ref, dg_ref, du_ref, *outs) = rest[:count], rest[count:]
     t = place_ref[1]
@@ -237,12 +236,12 @@
         for m in range(near):
             y_ref[m * cap : (m + 1) * cap, :] = refs[m][:cap, :]
     else:
-        put(y_ref, 0, t, tps, refs)
+        put(y_ref, t, at, refs)
     rows = y_ref.shape[0]
-    at = slice(first, first + rows)
+    here = slice(first, first + rows)
     d_act = dot(y_ref[...], down_ref[...], COLS)
-    dg = (d_act * slope_ref[at, :]).astype(BF16)
-    du = (d_act * swish_ref[at, :]).astype(BF16)
+    dg = (d_act * slope_ref[here, :]).astype(BF16)
+    du = (d_act * swish_ref[here, :]).astype(BF16)
     dg_ref[...] = dg
     du_ref[...] = du
     width = gate_ref.shape[0] // tps
@@ -287,10 +286,13 @@
         o[...] = (a if m < half else b)[i * cap : (i + 1) * cap, :]
 
 
-def grads_body(split, act_ref, x_ref, dg0_ref, du0_ref, y0_ref, dg1_ref, du1_ref, y1_ref, gg_ref, gu_ref, gd_ref):
+def inner_body(split, x_ref, dg0_ref, du0_ref, dg1_ref, du1_ref, gg_ref, gu_ref):
     x0, x1 = x_ref[:split, :], x_ref[split:, :]
     gg_ref[...] = (dot(x0, dg0_ref[...], ROWS) + dot(x1, dg1_ref[...], ROWS)).astype(BF16)
     gu_ref[...] = (dot(x0, du0_ref[...], ROWS) + dot(x1, du1_ref[...], ROWS)).astype(BF16)
+
+
+def outer_body(split, act_ref, y0_ref, y1_ref, gd_ref):
     a0, a1 = act_ref[:split, :], act_ref[split:, :]
     gd_ref[...] = (dot(a0, y0_ref[...], ROWS) + dot(a1, y1_ref[...], ROWS)).astype(BF16)
 
@@ -311,16 +313,19 @@
     out_ref[...] = dot(slots_ref[...], rows).astype(BF16)
 
 
-def mix_body(tps, place_ref, inv_ref, gain_ref, normed_ref, cot_ref, mat_ref, keep_ref, *rest):
+def ratio_body(inv_ref, gain_ref, normed_ref, out_ref):
+    out_ref[...] = column(inv_ref[...]) * normed_ref[...].astype(F32) / gain_ref[...]
+
+
+def mix_body(tps, place_ref, inv_ref, gain_ref, ratio_ref, normed_ref, cot_ref, mat_ref, keep_ref, *rest):
     pieces, (grad_ref, *strips, dn_ref, mix_ref) = rest[:tps], rest[tps:]
     s, t = place_ref[0], place_ref[1]
     for j in range(tps):
         dn_ref[:, wide(t ^ j, pieces[j].shape[1])] = pieces[j][...]
     dn = dn_ref[...].astype(F32)
     normed = normed_ref[...].astype(F32)
-    gain = gain_ref[...]
     stat = jnp.sum(dn * normed, axis=1, keepdims=True) * (1.0 / dn.shape[1])
-    mix = cot_ref[...].astype(F32) + column(inv_ref[...]) * (gain * dn - (normed / gain) * stat)
+    mix = cot_ref[...].astype(F32) + (column(inv_ref[...]) * gain_ref[...]) * dn - ratio_ref[...] * stat
     mix = mix.astype(BF16)
     mix_ref[...] = mix
     keep = keep_ref[...]
@@ -449,15 +454,30 @@
         edges = jnp.concatenate([edges, swap(edges, "sp", step)], axis=0)
         step *= 2
 
-    def spread(blocks):
+    def spread(blocks, first, direct):
         mine = call(
             functools.partial(join_body, cap), sds((len(blocks) * cap, width), BF16), *blocks
         )
-        return [mine] + [swap(mine, "tp", j) for j in range(1, tps)]
-
-    xp = spread(xs)
+        n = mine.shape[0]
+        if tps != 4 or direct:
+            pieces = [mine] + [swap(mine, "tp", j) for j in range(1, tps)]
+            return pieces, [(first, j) for j in range(tps)]
+        one, two = swap(mine, "tp", 1), swap(mine, "tp", 2)
+        low = swap(one[: n // 2], "tp", 2)
+        high = swap(two[n // 2 :], "tp", 1)
+        return [mine, one, two, low, high], [
+            (first, 0),
+            (first, 1),
+            (first, 2),
+            (first, 3),
+            (first + n // 2, 3),
+        ]
+
     half = far // 2
-    yp = spread(ys[:half]) + spread(ys[half:])
+    xp, at_x = spread(xs, near * cap, False)
+    yp, at_y = spread(ys[:half], 0, True)
+    wp, at_w = spread(ys[half:], half * cap, True)
+    yp, at_y = yp + wp, at_y + at_w
 
     hidden, kk, coef = call(
         functools.partial(enter_body, groups),
@@ -469,6 +489,8 @@
         edges,
         scalars=place,
     )
+    inverse, gains = inverse_root_mean_square[None, :], expert_norm_scale[None, :]
+    ratio = call(ratio_body, sds((tok, features), F32), inverse, gains, normed)
     slots = call(
         functools.partial(slots_body, groups, cap), sds((tok, rows), BF16), routes_t, scalars=place
     )
@@ -477,7 +499,7 @@
     thin_rows = sds((rows, hid), BF16)
     full_rows = sds((rows, features), BF16)
     act, swish, bend, x_all = call(
-        functools.partial(hidden_body, near, tps, cap),
+        functools.partial(hidden_body, near, cap, at_x),
         [thin_rows, wide_rows, wide_rows, full_rows],
         gate_w,
         up_w,
@@ -492,7 +514,7 @@
         piece = sds((n, width), BF16)
         keep_rows = sds((n, width), F32)
         return call(
-            functools.partial(back_body, first, 0 if first else near, tps, cap),
+            functools.partial(back_body, first, 0 if first else near, tps, cap, at_y),
             [sds((n, features), BF16), sds((n, hid), BF16), sds((n, hid), BF16)]
             + ([piece, piece, keep_rows, keep_rows] if tps == 4 else [piece] * tps),
             gate_w,
@@ -506,17 +528,17 @@
 
     y1, dg1, du1, *parts1 = back(near * cap, far, yp)
     y0, dg0, du0, *parts0 = back(0, near, close_y)
-    grads = call(
-        functools.partial(grads_body, near * cap),
-        [sds((features, hid), BF16), sds((features, hid), BF16), sds((hid, features), BF16)],
-        act,
+    grad_gate, grad_up = call(
+        functools.partial(inner_body, near * cap),
+        [sds((features, hid), BF16)] * 2,
         x_all,
         dg0,
         du0,
-        y0,
         dg1,
         du1,
-        y1,
+    )
+    grad_down = call(
+        functools.partial(outer_body, near * cap), sds((hid, features), BF16), act, y0, y1
     )
 
     def reduced(parts, count):
@@ -541,9 +563,11 @@
     summed = reduced(parts1, far)
     summed = list(reduced(parts0, near)) + list(summed)
     blocks = [summed[0]] + [swap(b, "sp", m) for m, b in enumerate(summed) if m]
-    grad_gate, grad_up, grad_down = grads
-    hid_even = jnp.concatenate(
-        [hidden] + [swap(hidden, "sp", m) for m in range(2, groups, 2)], axis=0
+    hid_even = call(
+        functools.partial(join_body, tok),
+        sds((groups // 2 * tok, chan), BF16),
+        hidden,
+        *[swap(hidden, "sp", m) for m in range(2, groups, 2)],
     )
     hid_odd = swap(hid_even, "sp", 1)
 
@@ -552,16 +576,18 @@
     strip = features // groups
     grad_loc, *strips = call(
         functools.partial(mix_body, tps),
-        [plane] + [sds((tok + 8, strip), BF16)] * groups + [sds((tok, features), BF16)] * 2,
-        inverse_root_mean_square[None, :],
-        expert_norm_scale[None, :],
+        [plane] + [sds((tok + 8, strip), BF16)] * groups,
+        inverse,
+        gains,
+        ratio,
         normed,
         cotangent,
         output_matrix,
         keep,
         *norms,
         scalars=place,
-    )[:-2]
+        scratch=[sds((tok, features), BF16)] * 2,
+    )
     strips = [strips[0]] + [swap(c, "sp", m) for m, c in enumerate(strips) if m]
     grad_out_weight, grad_rec, grad_decay, grad_input = call(
         functools.partial(final_body, groups, tok),

time: 126 us -> 136 us (1.079)
  waiting for transfers between devices: 32.4 us -> 48.6 us
  starting transfers between devices: 66.7 us -> 59.3 us
    ppermute x52 -> x53, waiting for transfers between devices: 32.4 us -> 48.6 us  [swap(): return lax.ppermute(x, axis, [(i, i ^ m) for i in range(n)])]
    ppermute x52 -> x53, starting transfers between devices: 66.7 us -> 59.3 us  [swap(): return lax.ppermute(x, axis, [(i, i ^ m) for i in range(n)])]
    pallas_call x20 -> x23, Pallas kernels: 23.5 us -> 23.8 us  [call(): pl.pallas_call(body, out_shape=outs, in_specs=ins, out_specs=jax.tree.map...]
  transfers between devices with their start and end apart: 52 -> 53, of which waited for: 15 -> 21; matrix products, arithmetic and copies ran while one was open for 2% -> 1% of each run, Pallas kernels for 16% -> 15%
where the time goes in v1:
time: 136 us; the launch traced here: 135 us
  starting transfers between devices  59.3 us (44%)
  waiting for transfers between devices  48.6 us (36%)
  Pallas kernels  23.8 us (18%)
  other arithmetic  1.97 us (1%)
    ppermute x53, starting transfers between devices, swap(): return lax.ppermute(x, axis, [(i, i ^ m) for i in range(n)])  59.3 us
    ppermute x53, waiting for transfers between devices, swap(): return lax.ppermute(x, axis, [(i, i ^ m) for i in range(n)])  48.6 us
    pallas_call x23, Pallas kernels, call(): pl.pallas_call(body, out_shape=outs, in_specs=ins, out_specs=jax.tree.map...  23.8 us
  transfers between devices with their start and end apart: 53, of which 21 were waited for; matrix products, arithmetic and copies ran while one was open for 1% of the time, Pallas kernels for 15%

profile of v1, /device:TPU:0, one launch (start us, length us, event | category | flops | bytes accessed | tf_op | source)
XLA Modules:
  0.0 134.7 jit_solution(6438095126786740542)
XLA Ops:
  0.7 2.0 %shard_map.198 = (bf16[64,512]{1,0:T(8,128)(2,1)S(1)}, bf16[64,512]{1,0:T(8,128)(2,1)S(1)}, bf16[64,512]{1,0:T(8,128)(2,1)S(1)}, bf16[64,512]{1,0:T(8,128)(2,1)S...) custom-call(s32[2]{0:T(128)S(1)} %pad_add_fusion.place_ref, ...), custom_call_target="tpu_custom_call" | custom-call | tf_op jit(solution)/shard_map/pallas_call | solution.py:27
  2.7 4.1 %collective-permute-start.3 = (bf16[64,512]{1,0:T(8,128)(2,1)S(1)}, bf16[64,512]{1,0:T(8,128)(2,1)S(1)}, u32[]{:S(2)}, u32[]{:S(2)}) collective-permute-start(bf16[64,512]{1,0:T(8,128)(2,1)S(1)} %get-tuple-element.112), channel_id=1, source_target_pairs={{0,16},{4,20},{8,24},{12,28},{16,0},{20,4},{24,8},{28,12},{1,17},{... | collective-permute-start | bytes 196616 | tf_op jit(solution)/shard_map/ppermute | solution.py:43
  6.8 3.1 %collective-permute-start.5 = (bf16[64,512]{1,0:T(8,128)(2,1)S(1)}, bf16[64,512]{1,0:T(8,128)(2,1)S(1)}, u32[]{:S(2)}, u32[]{:S(2)}) collective-permute-start(bf16[64,512]{1,0:T(8,128)(2,1)S(1)} %get-tuple-element.114), channel_id=1, source_target_pairs={{0,24},{4,28},{8,16},{12,20},{16,8},{20,12},{24,0},{28,4},{1,25},{... | collective-permute-start | bytes 196616 | tf_op jit(solution)/shard_map/ppermute | solution.py:43
  11.9 1.9 %collective-permute-start.14 = (bf16[64,512]{1,0:T(8,128)(2,1)S(1)}, bf16[64,512]{1,0:T(8,128)(2,1)S(1)}, u32[]{:S(2)}, u32[]{:S(2)}) collective-permute-start(bf16[64,512]{1,0:T(8,128)(2,1)S(1)} %get-tuple-element.124), channel_id=1, source_target_pairs={{0,20},{4,16},{8,28},{12,24},{16,4},{20,0},{24,12},{28,8},{1,21},{... | collective-permute-start | bytes 196616 | tf_op jit(solution)/shard_map/ppermute | solution.py:43
  15.2 2.0 %shard_map.200 = (bf16[136,2048]{1,0:T(8,128)(2,1)S(1)}, bf16[136,2048]{1,0:T(8,128)(2,1)S(1)}, bf16[72,2048]{1,0:T(8,128)(2,1)S(1)}, bf16[72,2048]{1,0:T(8,128)(2,1)S(1)}) custom-call(s32[2]{0:T(128)S(1)} %pad_add_fusion.place_ref, s32[2,128]{1,0:T(2,128)} %bitcast.23, f32[2,128]{1,0:T(2,128)} %bitcast.29, bf16[128,2048]{1,0:T(8,128)(2,1)} %normed_ref.7, ...), custom_call_target="tpu_custom_call" | custom-call | tf_op jit(solution)/shard_map/pallas_call | solution.py:27
  17.2 5.7 %collective-permute-done.13.refs_0_ = bf16[64,512]{1,0:T(8,128)(2,1)S(1)} collective-permute-done((bf16[64,512]{1,0:T(8,128)(2,1)S(1)}, bf16[64,512]{1,0:T(8,128)(2,1)S(1)}, u32[]{:S(2)}, u32[]{:S(2)}) %collective-permute-start.13) | collective-permute-done | bytes 65568 | tf_op jit(solution)/shard_map/ppermute | solution.py:43
  24.5 3.3 %collective-permute-start.18 = (bf16[64,512]{1,0:T(8,128)(2,1)S(1)}, bf16[64,512]{1,0:T(8,128)(2,1)S(1)}, u32[]{:S(2)}, u32[]{:S(2)}) collective-permute-start(bf16[64,512]{1,0:T(8,128)(2,1)S(1)} %get-tuple-element.125), channel_id=1, source_target_pairs={{0,24},{4,28},{8,16},{12,20},{16,8},{20,12},{24,0},{28,4},{1,25},{... | collective-permute-start | bytes 196616 | tf_op jit(solution)/shard_map/ppermute | solution.py:43
  32.5 4.4 %collective-permute-done.19.refs_1_ = bf16[64,512]{1,0:T(8,128)(2,1)S(1)} collective-permute-done((bf16[64,512]{1,0:T(8,128)(2,1)S(1)}, bf16[64,512]{1,0:T(8,128)(2,1)S(1)}, u32[]{:S(2)}, u32[]{:S(2)}) %collective-permute-start.19) | collective-permute-done | bytes 65568 | tf_op jit(solution)/shard_map/ppermute | solution.py:43
  39.9 4.3 %collective-permute-done.8.rest_6_ = bf16[256,512]{1,0:T(8,128)(2,1)S(1)} collective-permute-done((bf16[256,512]{1,0:T(8,128)(2,1)S(1)}, bf16[256,512]{1,0:T(8,128)(2,1)S(1)}, u32[]{:S(2)}, u32[]{:S(2)}) %collective-permute-start.8) | collective-permute-done | bytes 262176 | tf_op jit(solution)/shard_map/ppermute | solution.py:43
  45.4 3.5 %collective-permute-done.1.rest_2_ = bf16[64,2048]{1,0:T(8,128)(2,1)S(1)} collective-permute-done((bf16[64,2048]{1,0:T(8,128)(2,1)S(1)}, bf16[64,2048]{1,0:T(8,128)(2,1)S(1)}, u32[]{:S(2)}, u32[]{:S(2)}) %collective-permute-start.1) | collective-permute-done | bytes 262176 | tf_op jit(solution)/shard_map/ppermute | solution.py:43
  49.6 2.4 %collective-permute-done.2.rest_3_ = bf16[64,2048]{1,0:T(8,128)(2,1)S(1)} collective-permute-done((bf16[64,2048]{1,0:T(8,128)(2,1)S(1)}, bf16[64,2048]{1,0:T(8,128)(2,1)S(1)}, u32[]{:S(2)}, u32[]{:S(2)}) %collective-permute-start.2) | collective-permute-done | bytes 262176 | tf_op jit(solution)/shard_map/ppermute | solution.py:43
  54.6 2.4 %collective-permute-done.9.rest_7_ = bf16[128,512]{1,0:T(8,128)(2,1)S(1)} collective-permute-done((bf16[128,512]{1,0:T(8,128)(2,1)S(1)}, bf16[128,512]{1,0:T(8,128)(2,1)S(1)}, u32[]{:S(2)}, u32[]{:S(2)}) %collective-permute-start.9) | collective-permute-done | bytes 131104 | tf_op jit(solution)/shard_map/ppermute | solution.py:43
  59.0 3.2 %shard_map.202 = (bf16[512,512]{1,0:T(8,128)(2,1)S(1)}, f32[512,512]{1,0:T(8,128)S(1)}, f32[512,512]{1,0:T(8,128)S(1)}, bf16[512,2048]{1,0:T(8,128)(2,1)S(1)}) custom-call(s32[2]{0:T(128)S(1)} %pad_add_fusion.place_ref, bf16[2048,512]{1,0:T(8,128)(2,1)S(1)} %bitcast.12, bf16[2048,512]{1,0:T(8,128)(2,1)S(1)} %bitcast.15, ...), custom_call_target="tpu_custom_call" | custom-call | tf_op jit(solution)/shard_map/pallas_call | solution.py:27
  62.3 3.2 %collective-permute-done.21.rest_6_ = bf16[128,512]{1,0:T(8,128)(2,1)S(1)} collective-permute-done((bf16[128,512]{1,0:T(8,128)(2,1)S(1)}, bf16[128,512]{1,0:T(8,128)(2,1)S(1)}, u32[]{:S(2)}, u32[]{:S(2)}) %collective-permute-start.21) | collective-permute-done | bytes 131104 | tf_op jit(solution)/shard_map/ppermute | solution.py:43
  65.5 2.5 %shard_map.206 = (bf16[256,2048]{1,0:T(8,128)(2,1)S(1)}, bf16[256,512]{1,0:T(8,128)(2,1)S(1)}, bf16[256,512]{1,0:T(8,128)(2,1)S(1)}, bf16[256,512]{1,0:T(8,128)(...) custom-call(s32[2]{0:T(128)S(1)} %pad_add_fusion.place_ref, ...), custom_call_target="tpu_custom_call" | custom-call | tf_op jit(solution)/shard_map/pallas_call | solution.py:27
  69.2 2.5 %shard_map.203 = (bf16[256,2048]{1,0:T(8,128)(2,1)S(1)}, bf16[256,512]{1,0:T(8,128)(2,1)S(1)}, bf16[256,512]{1,0:T(8,128)(2,1)S(1)}, bf16[256,512]{1,0:T(8,128)(...) custom-call(s32[2]{0:T(128)S(1)} %pad_add_fusion.place_ref, ...), custom_call_target="tpu_custom_call" | custom-call | tf_op jit(solution)/shard_map/pallas_call | solution.py:27
  74.7 2.1 %collective-permute-start.23 = (bf16[32,256]{1,0:T(8,128)(2,1)S(1)}, bf16[32,256]{1,0:T(8,128)(2,1)S(1)}, u32[]{:S(2)}, u32[]{:S(2)}) collective-permute-start(bf16[32,256]{1,0:T(8,128)(2,1)S(1)} %shard_map.209), channel_id=1, source_target_pairs={{0,16},{4,20},{8,24},{12,28},{16,0},{20,4},{24,8},{28,12},{1,17},{... | collective-permute-start | bytes 49160 | tf_op jit(solution)/shard_map/ppermute | solution.py:43
  79.9 2.9 %collective-permute-done.24.got_a = bf16[256,512]{1,0:T(8,128)(2,1)S(1)} collective-permute-done((bf16[256,512]{1,0:T(8,128)(2,1)S(1)}, bf16[256,512]{1,0:T(8,128)(2,1)S(1)}, u32[]{:S(2)}, u32[]{:S(2)}) %collective-permute-start.24) | collective-permute-done | bytes 262176 | tf_op jit(solution)/shard_map/ppermute | solution.py:43
  86.3 1.9 %collective-permute-start.42 = (bf16[128,256]{1,0:T(8,128)(2,1)S(1)}, bf16[128,256]{1,0:T(8,128)(2,1)S(1)}, u32[]{:S(2)}, u32[]{:S(2)}) collective-permute-start(bf16[128,256]{1,0:T(8,128)(2,1)S(1)} %get-tuple-element.164.refs_0_), channel_id=1, source_target_pairs={{0,8},{4,12},{8,0},{12,4},{16,24},{20,28},{24,16},{28,20},{1,9},{5... | collective-permute-start | bytes 196616 | tf_op jit(solution)/shard_map/ppermute | solution.py:43
  88.8 1.9 %collective-permute-start.44 = (bf16[128,256]{1,0:T(8,128)(2,1)S(1)}, bf16[128,256]{1,0:T(8,128)(2,1)S(1)}, u32[]{:S(2)}, u32[]{:S(2)}) collective-permute-start(bf16[128,256]{1,0:T(8,128)(2,1)S(1)} %get-tuple-element.164.refs_0_), channel_id=1, source_target_pairs={{0,24},{4,28},{8,16},{12,20},{16,8},{20,12},{24,0},{28,4},{1,25},{... | collective-permute-start | bytes 196616 | tf_op jit(solution)/shard_map/ppermute | solution.py:43
  90.8 2.9 %collective-permute-start.35 = (bf16[64,512]{1,0:T(8,128)(2,1)S(1)}, bf16[64,512]{1,0:T(8,128)(2,1)S(1)}, u32[]{:S(2)}, u32[]{:S(2)}) collective-permute-start(bf16[64,512]{1,0:T(8,128)(2,1)S(1)} %get-tuple-element.157), channel_id=1, source_target_pairs={{0,16},{4,20},{8,24},{12,28},{16,0},{20,4},{24,8},{28,12},{1,17},{... | collective-permute-start | bytes 196616 | tf_op jit(solution)/shard_map/ppermute | solution.py:43
  93.7 1.8 %collective-permute-start.37 = (bf16[64,512]{1,0:T(8,128)(2,1)S(1)}, bf16[64,512]{1,0:T(8,128)(2,1)S(1)}, u32[]{:S(2)}, u32[]{:S(2)}) collective-permute-start(bf16[64,512]{1,0:T(8,128)(2,1)S(1)} %get-tuple-element.159), channel_id=1, source_target_pairs={{0,24},{4,28},{8,16},{12,20},{16,8},{20,12},{24,0},{28,4},{1,25},{... | collective-permute-start | bytes 196616 | tf_op jit(solution)/shard_map/ppermute | solution.py:43
  95.6 1.6 %collective-permute-start.38 = (bf16[64,512]{1,0:T(8,128)(2,1)S(1)}, bf16[64,512]{1,0:T(8,128)(2,1)S(1)}, u32[]{:S(2)}, u32[]{:S(2)}) collective-permute-start(bf16[64,512]{1,0:T(8,128)(2,1)S(1)} %get-tuple-element.160), channel_id=1, source_target_pairs={{0,28},{4,24},{8,20},{12,16},{16,12},{20,8},{24,4},{28,0},{1,29},{... | collective-permute-start | bytes 196616 | tf_op jit(solution)/shard_map/ppermute | solution.py:43
  97.9 3.9 %collective-permute-done.35.rest_4_ = bf16[64,512]{1,0:T(8,128)(2,1)S(1)} collective-permute-done((bf16[64,512]{1,0:T(8,128)(2,1)S(1)}, bf16[64,512]{1,0:T(8,128)(2,1)S(1)}, u32[]{:S(2)}, u32[]{:S(2)}) %collective-permute-start.35) | collective-permute-done | bytes 65568 | tf_op jit(solution)/shard_map/ppermute | solution.py:43
  107.7 1.9 %collective-permute-start.40 = (bf16[128,512]{1,0:T(8,128)(2,1)S(1)}, bf16[128,512]{1,0:T(8,128)(2,1)S(1)}, u32[]{:S(2)}, u32[]{:S(2)}) collective-permute-start(bf16[128,512]{1,0:T(8,128)(2,1)S(1)} %shard_map.217.rest_0_), channel_id=1, source_target_pairs={{0,2},{1,3},{2,0},{3,1},{4,6},{5,7},{6,4},{7,5},{8,10},{9,11},{10,... | collective-permute-start | bytes 393224 | tf_op jit(solution)/shard_map/ppermute | solution.py:43
  111.3 2.7 %collective-permute-done.39.rest_1_ = bf16[128,512]{1,0:T(8,128)(2,1)S(1)} collective-permute-done((bf16[128,512]{1,0:T(8,128)(2,1)S(1)}, bf16[128,512]{1,0:T(8,128)(2,1)S(1)}, u32[]{:S(2)}, u32[]{:S(2)}) %collective-permute-start.39) | collective-permute-done | bytes 131104 | tf_op jit(solution)/shard_map/ppermute | solution.py:43
  115.6 1.8 %collective-permute-done.41.rest_3_ = bf16[128,512]{1,0:T(8,128)(2,1)S(1)} collective-permute-done((bf16[128,512]{1,0:T(8,128)(2,1)S(1)}, bf16[128,512]{1,0:T(8,128)(2,1)S(1)}, u32[]{:S(2)}, u32[]{:S(2)}) %collective-permute-start.41) | collective-permute-done | bytes 131104 | tf_op jit(solution)/shard_map/ppermute | solution.py:43
  119.1 1.8 %collective-permute-start.48 = (bf16[136,256]{1,0:T(8,128)(2,1)S(1)}, bf16[136,256]{1,0:T(8,128)(2,1)S(1)}, u32[]{:S(2)}, u32[]{:S(2)}) collective-permute-start(bf16[136,256]{1,0:T(8,128)(2,1)S(1)} %get-tuple-element.168), channel_id=1, source_target_pairs={{0,12},{4,8},{8,4},{12,0},{16,28},{20,24},{24,20},{28,16},{1,13},{... | collective-permute-start | bytes 208904 | tf_op jit(solution)/shard_map/ppermute | solution.py:43
  121.3 2.1 %collective-permute-start.50 = (bf16[136,256]{1,0:T(8,128)(2,1)S(1)}, bf16[136,256]{1,0:T(8,128)(2,1)S(1)}, u32[]{:S(2)}, u32[]{:S(2)}) collective-permute-start(bf16[136,256]{1,0:T(8,128)(2,1)S(1)} %get-tuple-element.170), channel_id=1, source_target_pairs={{0,20},{4,16},{8,28},{12,24},{16,4},{20,0},{24,12},{28,8},{1,21},{... | collective-permute-start | bytes 208904 | tf_op jit(solution)/shard_map/ppermute | solution.py:43
  125.0 2.1 %collective-permute-start.52 = (bf16[136,256]{1,0:T(8,128)(2,1)S(1)}, bf16[136,256]{1,0:T(8,128)(2,1)S(1)}, u32[]{:S(2)}, u32[]{:S(2)}) collective-permute-start(bf16[136,256]{1,0:T(8,128)(2,1)S(1)} %get-tuple-element.172), channel_id=1, source_target_pairs={{0,28},{4,24},{8,20},{12,16},{16,12},{20,8},{24,4},{28,0},{1,29},{... | collective-permute-start | bytes 208904 | tf_op jit(solution)/shard_map/ppermute | solution.py:43
  127.1 2.6 %shard_map.208 = bf16[512,2048]{1,0:T(8,128)(2,1)} custom-call(bf16[512,512]{1,0:T(8,128)(2,1)S(1)} %get-tuple-element.131.act_ref, bf16[256,2048]{1,0:T(8,128)(2,1)S(1)} %get-tuple-element.132.y0_ref, bf16[256,2048]{1,0:T(8,128)(2,1)S(1)} %get-tuple-element.133.y1_ref), custom_call_target="tpu_custom_call" | custom-call | tf_op jit(solution)/shard_map/pallas_call | solution.py:27
  129.7 3.7 %shard_map.207 = (bf16[2048,512]{1,0:T(8,128)(2,1)}, bf16[2048,512]{1,0:T(8,128)(2,1)}) custom-call(bf16[512,2048]{1,0:T(8,128)(2,1)S(1)} %get-tuple-element.116.x_ref, bf16[256,512]{1,0:T(8,128)(2,1)S(1)} %get-tuple-element.121.dg0_ref, bf16[256,512]{1,0:T(8,128)(2,1)S(1)} %get-tuple-element.122.du0_ref, bf16[256,512]{1,0:T(8,128)(2,1)S(1)} %get-tuple-element.127.dg1_ref, ...), custom_call_target="tpu_custom_call" | custom-call | tf_op jit(solution)/shard_map/pallas_call | solution.py:27
  (121 shorter events, 45.6 us)
Async XLA Ops:
  2.7 9.2 %collective-permute-start.3 = (bf16[64,512]{1,0:T(8,128)(2,1)S(1)}, bf16[64,512]{1,0:T(8,128)(2,1)S(1)}, u32[]{:S(2)}, u32[]{:S(2)}) collective-permute-start(bf16[64,512]{1,0:T(8,128)(2,1)S(1)} %get-tuple-element.112), channel_id=1, source_target_pairs={{0,16},{4,20},{8,24},{12,28},{16,0},{20,4},{24,8},{28,12},{1,17},{... | collective-permute-start | bytes 196616 | tf_op jit(solution)/shard_map/ppermute | solution.py:43
  6.8 21.0 %collective-permute-start.4 = (bf16[64,512]{1,0:T(8,128)(2,1)S(1)}, bf16[64,512]{1,0:T(8,128)(2,1)S(1)}, u32[]{:S(2)}, u32[]{:S(2)}) collective-permute-start(bf16[64,512]{1,0:T(8,128)(2,1)S(1)} %get-tuple-element.113), channel_id=1, source_target_pairs={{0,20},{4,16},{8,28},{12,24},{16,4},{20,0},{24,12},{28,8},{1,21},{... | collective-permute-start | bytes 196616 | tf_op jit(solution)/shard_map/ppermute | solution.py:43
  6.8 22.5 %collective-permute-start.5 = (bf16[64,512]{1,0:T(8,128)(2,1)S(1)}, bf16[64,512]{1,0:T(8,128)(2,1)S(1)}, u32[]{:S(2)}, u32[]{:S(2)}) collective-permute-start(bf16[64,512]{1,0:T(8,128)(2,1)S(1)} %get-tuple-element.114), channel_id=1, source_target_pairs={{0,24},{4,28},{8,16},{12,20},{16,8},{20,12},{24,0},{28,4},{1,25},{... | collective-permute-start | bytes 196616 | tf_op jit(solution)/shard_map/ppermute | solution.py:43
  9.9 20.9 %collective-permute-start.6 = (bf16[64,512]{1,0:T(8,128)(2,1)S(1)}, bf16[64,512]{1,0:T(8,128)(2,1)S(1)}, u32[]{:S(2)}, u32[]{:S(2)}) collective-permute-start(bf16[64,512]{1,0:T(8,128)(2,1)S(1)} %get-tuple-element.115), channel_id=1, source_target_pairs={{0,28},{4,24},{8,20},{12,16},{16,12},{20,8},{24,4},{28,0},{1,29},{... | collective-permute-start | bytes 196616 | tf_op jit(solution)/shard_map/ppermute | solution.py:43
  10.5 12.4 %collective-permute-start.13 = (bf16[64,512]{1,0:T(8,128)(2,1)S(1)}, bf16[64,512]{1,0:T(8,128)(2,1)S(1)}, u32[]{:S(2)}, u32[]{:S(2)}) collective-permute-start(bf16[64,512]{1,0:T(8,128)(2,1)S(1)} %get-tuple-element.123), channel_id=1, source_target_pairs={{0,16},{4,20},{8,24},{12,28},{16,0},{20,4},{24,8},{28,12},{1,17},{... | collective-permute-start | bytes 196616 | tf_op jit(solution)/shard_map/ppermute | solution.py:43
  11.9 12.6 %collective-permute-start.14 = (bf16[64,512]{1,0:T(8,128)(2,1)S(1)}, bf16[64,512]{1,0:T(8,128)(2,1)S(1)}, u32[]{:S(2)}, u32[]{:S(2)}) collective-permute-start(bf16[64,512]{1,0:T(8,128)(2,1)S(1)} %get-tuple-element.124), channel_id=1, source_target_pairs={{0,20},{4,16},{8,28},{12,24},{16,4},{20,0},{24,12},{28,8},{1,21},{... | collective-permute-start | bytes 196616 | tf_op jit(solution)/shard_map/ppermute | solution.py:43
  22.9 34.6 %collective-permute-start = (bf16[136,2048]{1,0:T(8,128)(2,1)S(1)}, bf16[136,2048]{1,0:T(8,128)(2,1)S(1)}, u32[]{:S(2)}, u32[]{:S(2)}) collective-permute-start(bf16[136,2048]{1,0:T(8,128)(2,1)S(1)} %get-tuple-element.109), channel_id=1, source_target_pairs={{0,4},{4,0},{8,12},{12,8},{16,20},{20,16},{24,28},{28,24},{1,5},{5... | collective-permute-start | bytes 1671176 | tf_op jit(solution)/shard_map/ppermute | solution.py:43
  27.8 10.5 %collective-permute-start.15 = (bf16[128,512]{1,0:T(8,128)(2,1)S(1)}, bf16[128,512]{1,0:T(8,128)(2,1)S(1)}, u32[]{:S(2)}, u32[]{:S(2)}) collective-permute-start(bf16[128,512]{1,0:T(8,128)(2,1)S(1)} %shard_map.204.rest_0_), channel_id=1, source_target_pairs={{0,1},{1,0},{2,3},{3,2},{4,5},{5,4},{6,7},{7,6},{8,9},{9,8},{10,11... | collective-permute-start | bytes 393224 | tf_op jit(solution)/shard_map/ppermute | solution.py:43
  29.3 10.5 %collective-permute-start.16 = (bf16[128,512]{1,0:T(8,128)(2,1)S(1)}, bf16[128,512]{1,0:T(8,128)(2,1)S(1)}, u32[]{:S(2)}, u32[]{:S(2)}) collective-permute-start(bf16[128,512]{1,0:T(8,128)(2,1)S(1)} %shard_map.204.rest_0_), channel_id=1, source_target_pairs={{0,2},{1,3},{2,0},{3,1},{4,6},{5,7},{6,4},{7,5},{8,10},{9,11},{10,... | collective-permute-start | bytes 393224 | tf_op jit(solution)/shard_map/ppermute | solution.py:43
  30.8 9.0 %collective-permute-start.17 = (bf16[128,512]{1,0:T(8,128)(2,1)S(1)}, bf16[128,512]{1,0:T(8,128)(2,1)S(1)}, u32[]{:S(2)}, u32[]{:S(2)}) collective-permute-start(bf16[128,512]{1,0:T(8,128)(2,1)S(1)} %shard_map.204.rest_0_), channel_id=1, source_target_pairs={{0,3},{1,2},{2,1},{3,0},{4,7},{5,6},{6,5},{7,4},{8,11},{9,10},{10,... | collective-permute-start | bytes 393224 | tf_op jit(solution)/shard_map/ppermute | solution.py:43
  39.8 9.2 %collective-permute-start.1 = (bf16[64,2048]{1,0:T(8,128)(2,1)S(1)}, bf16[64,2048]{1,0:T(8,128)(2,1)S(1)}, u32[]{:S(2)}, u32[]{:S(2)}) collective-permute-start(bf16[64,2048]{1,0:T(8,128)(2,1)S(1)} %get-tuple-element.110), channel_id=1, source_target_pairs={{0,8},{4,12},{8,0},{12,4},{16,24},{20,28},{24,16},{28,20},{1,9},{5... | collective-permute-start | bytes 786440 | tf_op jit(solution)/shard_map/ppermute | solution.py:43
  39.8 12.2 %collective-permute-start.2 = (bf16[64,2048]{1,0:T(8,128)(2,1)S(1)}, bf16[64,2048]{1,0:T(8,128)(2,1)S(1)}, u32[]{:S(2)}, u32[]{:S(2)}) collective-permute-start(bf16[64,2048]{1,0:T(8,128)(2,1)S(1)} %get-tuple-element.111), channel_id=1, source_target_pairs={{0,12},{4,8},{8,4},{12,0},{16,28},{20,24},{24,20},{28,16},{1,13},{... | collective-permute-start | bytes 786440 | tf_op jit(solution)/shard_map/ppermute | solution.py:43
  44.2 25.0 %collective-permute-start.11 = (bf16[72,2048]{1,0:T(8,128)(2,1)S(1)}, bf16[72,2048]{1,0:T(8,128)(2,1)S(1)}, u32[]{:S(2)}, u32[]{:S(2)}) collective-permute-start(bf16[72,2048]{1,0:T(8,128)(2,1)S(1)} %get-tuple-element.119), channel_id=1, source_target_pairs={{0,8},{4,12},{8,0},{12,4},{16,24},{20,28},{24,16},{28,20},{1,9},{5... | collective-permute-start | bytes 884744 | tf_op jit(solution)/shard_map/ppermute | solution.py:43
  45.4 23.8 %collective-permute-start.12 = (bf16[72,2048]{1,0:T(8,128)(2,1)S(1)}, bf16[72,2048]{1,0:T(8,128)(2,1)S(1)}, u32[]{:S(2)}, u32[]{:S(2)}) collective-permute-start(bf16[72,2048]{1,0:T(8,128)(2,1)S(1)} %get-tuple-element.120), channel_id=1, source_target_pairs={{0,12},{4,8},{8,4},{12,0},{16,28},{20,24},{24,20},{28,16},{1,13},{... | collective-permute-start | bytes 884744 | tf_op jit(solution)/shard_map/ppermute | solution.py:43
  68.0 9.2 %collective-permute-start.31 = (bf16[256,512]{1,0:T(8,128)(2,1)S(1)}, bf16[256,512]{1,0:T(8,128)(2,1)S(1)}, u32[]{:S(2)}, u32[]{:S(2)}) collective-permute-start(bf16[256,512]{1,0:T(8,128)(2,1)S(1)} %get-tuple-element.151), channel_id=1, source_target_pairs={{0,1},{1,0},{2,3},{3,2},{4,5},{5,4},{6,7},{7,6},{8,9},{9,8},{10,11... | collective-permute-start | bytes 786440 | tf_op jit(solution)/shard_map/ppermute | solution.py:43
  68.7 9.2 %collective-permute-start.32 = (bf16[256,512]{1,0:T(8,128)(2,1)S(1)}, bf16[256,512]{1,0:T(8,128)(2,1)S(1)}, u32[]{:S(2)}, u32[]{:S(2)}) collective-permute-start(bf16[256,512]{1,0:T(8,128)(2,1)S(1)} %get-tuple-element.152), channel_id=1, source_target_pairs={{0,2},{1,3},{2,0},{3,1},{4,6},{5,7},{6,4},{7,5},{8,10},{9,11},{10,... | collective-permute-start | bytes 786440 | tf_op jit(solution)/shard_map/ppermute | solution.py:43
  71.7 11.2 %collective-permute-start.24 = (bf16[256,512]{1,0:T(8,128)(2,1)S(1)}, bf16[256,512]{1,0:T(8,128)(2,1)S(1)}, u32[]{:S(2)}, u32[]{:S(2)}) collective-permute-start(bf16[256,512]{1,0:T(8,128)(2,1)S(1)} %get-tuple-element.139), channel_id=1, source_target_pairs={{0,1},{1,0},{2,3},{3,2},{4,5},{5,4},{6,7},{7,6},{8,9},{9,8},{10,11... | collective-permute-start | bytes 786440 | tf_op jit(solution)/shard_map/ppermute | solution.py:43
  73.1 10.4 %collective-permute-start.25 = (bf16[256,512]{1,0:T(8,128)(2,1)S(1)}, bf16[256,512]{1,0:T(8,128)(2,1)S(1)}, u32[]{:S(2)}, u32[]{:S(2)}) collective-permute-start(bf16[256,512]{1,0:T(8,128)(2,1)S(1)} %get-tuple-element.140), channel_id=1, source_target_pairs={{0,2},{1,3},{2,0},{3,1},{4,6},{5,7},{6,4},{7,5},{8,10},{9,11},{10,... | collective-permute-start | bytes 786440 | tf_op jit(solution)/shard_map/ppermute | solution.py:43
  74.7 10.9 %collective-permute-start.23 = (bf16[32,256]{1,0:T(8,128)(2,1)S(1)}, bf16[32,256]{1,0:T(8,128)(2,1)S(1)}, u32[]{:S(2)}, u32[]{:S(2)}) collective-permute-start(bf16[32,256]{1,0:T(8,128)(2,1)S(1)} %shard_map.209), channel_id=1, source_target_pairs={{0,16},{4,20},{8,24},{12,28},{16,0},{20,4},{24,8},{28,12},{1,17},{... | collective-permute-start | bytes 49160 | tf_op jit(solution)/shard_map/ppermute | solution.py:43
  78.0 10.2 %collective-permute-start.33 = (bf16[128,512]{1,0:T(8,128)(2,1)S(1)}, bf16[128,512]{1,0:T(8,128)(2,1)S(1)}, u32[]{:S(2)}, u32[]{:S(2)}) collective-permute-start(bf16[128,512]{1,0:T(8,128)(2,1)S(1)} %get-tuple-element.155), channel_id=1, source_target_pairs={{0,2},{1,3},{2,0},{3,1},{4,6},{5,7},{6,4},{7,5},{8,10},{9,11},{10,... | collective-permute-start | bytes 393224 | tf_op jit(solution)/shard_map/ppermute | solution.py:43
  78.6 10.3 %collective-permute-start.34 = (bf16[128,512]{1,0:T(8,128)(2,1)S(1)}, bf16[128,512]{1,0:T(8,128)(2,1)S(1)}, u32[]{:S(2)}, u32[]{:S(2)}) collective-permute-start(bf16[128,512]{1,0:T(8,128)(2,1)S(1)} %get-tuple-element.156), channel_id=1, source_target_pairs={{0,1},{1,0},{2,3},{3,2},{4,5},{5,4},{6,7},{7,6},{8,9},{9,8},{10,11... | collective-permute-start | bytes 393224 | tf_op jit(solution)/shard_map/ppermute | solution.py:43
  83.7 10.0 %collective-permute-start.26 = (bf16[128,512]{1,0:T(8,128)(2,1)S(1)}, bf16[128,512]{1,0:T(8,128)(2,1)S(1)}, u32[]{:S(2)}, u32[]{:S(2)}) collective-permute-start(bf16[128,512]{1,0:T(8,128)(2,1)S(1)} %get-tuple-element.143), channel_id=1, source_target_pairs={{0,2},{1,3},{2,0},{3,1},{4,6},{5,7},{6,4},{7,5},{8,10},{9,11},{10,... | collective-permute-start | bytes 393224 | tf_op jit(solution)/shard_map/ppermute | solution.py:43
  84.2 9.5 %collective-permute-start.27 = (bf16[128,512]{1,0:T(8,128)(2,1)S(1)}, bf16[128,512]{1,0:T(8,128)(2,1)S(1)}, u32[]{:S(2)}, u32[]{:S(2)}) collective-permute-start(bf16[128,512]{1,0:T(8,128)(2,1)S(1)} %get-tuple-element.144), channel_id=1, source_target_pairs={{0,1},{1,0},{2,3},{3,2},{4,5},{5,4},{6,7},{7,6},{8,9},{9,8},{10,11... | collective-permute-start | bytes 393224 | tf_op jit(solution)/shard_map/ppermute | solution.py:43
  90.8 10.9 %collective-permute-start.35 = (bf16[64,512]{1,0:T(8,128)(2,1)S(1)}, bf16[64,512]{1,0:T(8,128)(2,1)S(1)}, u32[]{:S(2)}, u32[]{:S(2)}) collective-permute-start(bf16[64,512]{1,0:T(8,128)(2,1)S(1)} %get-tuple-element.157), channel_id=1, source_target_pairs={{0,16},{4,20},{8,24},{12,28},{16,0},{20,4},{24,8},{28,12},{1,17},{... | collective-permute-start | bytes 196616 | tf_op jit(solution)/shard_map/ppermute | solution.py:43
  93.7 9.5 %collective-permute-start.36 = (bf16[64,512]{1,0:T(8,128)(2,1)S(1)}, bf16[64,512]{1,0:T(8,128)(2,1)S(1)}, u32[]{:S(2)}, u32[]{:S(2)}) collective-permute-start(bf16[64,512]{1,0:T(8,128)(2,1)S(1)} %get-tuple-element.158), channel_id=1, source_target_pairs={{0,20},{4,16},{8,28},{12,24},{16,4},{20,0},{24,12},{28,8},{1,21},{... | collective-permute-start | bytes 196616 | tf_op jit(solution)/shard_map/ppermute | solution.py:43
  93.7 9.5 %collective-permute-start.37 = (bf16[64,512]{1,0:T(8,128)(2,1)S(1)}, bf16[64,512]{1,0:T(8,128)(2,1)S(1)}, u32[]{:S(2)}, u32[]{:S(2)}) collective-permute-start(bf16[64,512]{1,0:T(8,128)(2,1)S(1)} %get-tuple-element.159), channel_id=1, source_target_pairs={{0,24},{4,28},{8,16},{12,20},{16,8},{20,12},{24,0},{28,4},{1,25},{... | collective-permute-start | bytes 196616 | tf_op jit(solution)/shard_map/ppermute | solution.py:43
  95.6 9.2 %collective-permute-start.38 = (bf16[64,512]{1,0:T(8,128)(2,1)S(1)}, bf16[64,512]{1,0:T(8,128)(2,1)S(1)}, u32[]{:S(2)}, u32[]{:S(2)}) collective-permute-start(bf16[64,512]{1,0:T(8,128)(2,1)S(1)} %get-tuple-element.160), channel_id=1, source_target_pairs={{0,28},{4,24},{8,20},{12,16},{16,12},{20,8},{24,4},{28,0},{1,29},{... | collective-permute-start | bytes 196616 | tf_op jit(solution)/shard_map/ppermute | solution.py:43
  103.2 18.1 %collective-permute-start.45 = (bf16[512,256]{1,0:T(8,128)(2,1)S(1)}, bf16[512,256]{1,0:T(8,128)(2,1)S(1)}, u32[]{:S(2)}, u32[]{:S(2)}) collective-permute-start(bf16[512,256]{1,0:T(8,128)(2,1)S(1)} %shard_map.219.hid_even_ref), channel_id=1, source_target_pairs={{0,4},{4,0},{8,12},{12,8},{16,20},{20,16},{24,28},{28,24},{1,5},{5... | collective-permute-start | bytes 786440 | tf_op jit(solution)/shard_map/ppermute | solution.py:43
  119.1 14.3 %collective-permute-start.48 = (bf16[136,256]{1,0:T(8,128)(2,1)S(1)}, bf16[136,256]{1,0:T(8,128)(2,1)S(1)}, u32[]{:S(2)}, u32[]{:S(2)}) collective-permute-start(bf16[136,256]{1,0:T(8,128)(2,1)S(1)} %get-tuple-element.168), channel_id=1, source_target_pairs={{0,12},{4,8},{8,4},{12,0},{16,28},{20,24},{24,20},{28,16},{1,13},{... | collective-permute-start | bytes 208904 | tf_op jit(solution)/shard_map/ppermute | solution.py:43
  120.9 12.5 %collective-permute-start.49 = (bf16[136,256]{1,0:T(8,128)(2,1)S(1)}, bf16[136,256]{1,0:T(8,128)(2,1)S(1)}, u32[]{:S(2)}, u32[]{:S(2)}) collective-permute-start(bf16[136,256]{1,0:T(8,128)(2,1)S(1)} %get-tuple-element.169), channel_id=1, source_target_pairs={{0,16},{4,20},{8,24},{12,28},{16,0},{20,4},{24,8},{28,12},{1,17},{... | collective-permute-start | bytes 208904 | tf_op jit(solution)/shard_map/ppermute | solution.py:43
  121.3 12.1 %collective-permute-start.50 = (bf16[136,256]{1,0:T(8,128)(2,1)S(1)}, bf16[136,256]{1,0:T(8,128)(2,1)S(1)}, u32[]{:S(2)}, u32[]{:S(2)}) collective-permute-start(bf16[136,256]{1,0:T(8,128)(2,1)S(1)} %get-tuple-element.170), channel_id=1, source_target_pairs={{0,20},{4,16},{8,28},{12,24},{16,4},{20,0},{24,12},{28,8},{1,21},{... | collective-permute-start | bytes 208904 | tf_op jit(solution)/shard_map/ppermute | solution.py:43
  123.5 9.9 %collective-permute-start.51 = (bf16[136,256]{1,0:T(8,128)(2,1)S(1)}, bf16[136,256]{1,0:T(8,128)(2,1)S(1)}, u32[]{:S(2)}, u32[]{:S(2)}) collective-permute-start(bf16[136,256]{1,0:T(8,128)(2,1)S(1)} %get-tuple-element.171), channel_id=1, source_target_pairs={{0,24},{4,28},{8,16},{12,20},{16,8},{20,12},{24,0},{28,4},{1,25},{... | collective-permute-start | bytes 208904 | tf_op jit(solution)/shard_map/ppermute | solution.py:43
  (30 other events, 416.2 us)
